TPU v7x, 256 devices: a whole 4x4x8 slice. The times are simulated.
256 devices in a mesh: ep: 16 (over y, x), tp: 16 (over z, core).
Axes of the slice: x: 4, y: 4, z: 8, core: 2. Of those that a mesh axis runs over, the one named last changes fastest.
Arguments:
- hidden_in: bfloat16 [512, 4096], P('ep'), may hold values from -6 to 6
- mix_gain: float32 [4096], replicated, may hold values from 0.1 to 1.9
- w_query: bfloat16 [4096, 2048], P('ep', 'tp'), may hold values from -0.09375 to 0.09375
- w_key: bfloat16 [4096, 2048], P('ep', 'tp'), may hold values from -0.09375 to 0.09375
- w_value: bfloat16 [4096, 2048], P('ep', 'tp'), may hold values from -0.09375 to 0.09375
- w_outgate: bfloat16 [4096, 2048], P('ep', 'tp'), may hold values from -0.09375 to 0.09375
- w_gates: bfloat16 [2, 4096, 32], P(None, None, 'tp'), may hold values from -0.09375 to 0.09375
- gate_bias: float32 [2, 32], P(None, 'tp'), may hold values from -1 to 4
- state_matrix: float32 [512, 32, 64, 64], P('ep', 'tp'), may hold values from -2 to 2
- state_norm: float32 [512, 32, 64], P('ep', 'tp'), may hold values from -2 to 2
- state_max: float32 [512, 32], P('ep', 'tp'), may hold values from -3 to 3
- w_mix_out: bfloat16 [2048, 4096], P('tp'), may hold values from -0.125 to 0.125
- ffn_gain: float32 [4096], replicated, may hold values from 0.1 to 1.9
- routes: int32 [512, 2], replicated, may hold values from 0 to 31, all different within a row; in each aligned block of 32 rows (0 to 31, 32 to 63, ...) at most 3 rows name the same one
- route_weights: float32 [512, 2], P('ep'), may hold values from 0.1 to 1
- expert_gate: bfloat16 [32, 4096, 2048], P('ep', None, 'tp'), may hold values from -0.09375 to 0.09375
- expert_up: bfloat16 [32, 4096, 2048], P('ep', None, 'tp'), may hold values from -0.09375 to 0.09375
- expert_down: bfloat16 [32, 2048, 4096], P('ep', 'tp'), may hold values from -0.125 to 0.125
- shared_gate: bfloat16 [4096, 1024], P(None, 'tp'), may hold values from -0.09375 to 0.09375
- shared_up: bfloat16 [4096, 1024], P(None, 'tp'), may hold values from -0.09375 to 0.09375
- shared_down: bfloat16 [1024, 4096], P('tp'), may hold values from -0.1875 to 0.1875
Outputs:
- result: bfloat16 [512, 4096], P('ep', 'tp')
- new_matrix: float32 [512, 32, 64, 64], P('ep', 'tp')
- new_norm: float32 [512, 32, 64], P('ep', 'tp')
- new_max: float32 [512, 32], P('ep', 'tp')
Inputs may be any that keep to these rules, and one draw needn't show every extreme that they name: `routes`: each row names 2 different experts. In each aligned block of 32 rows (the rows of one device group along ep) no expert is named by more than 3 rows, a bound that some block reaches.
All inputs are finite; a program needn't handle non-finite values.
Results may differ from a plain program's by a relative error of at most 0.023.
Values may be sent and summed in bfloat16 or wider, within the bound.
A program may use at most 64 MiB of HBM per device.

v0:
```python
import jax
import jax.numpy as jnp
from jax import lax
from jax.sharding import PartitionSpec as P

norm_eps = 1e-06


def cut_along(x, dim, peers):
    dims = x.shape
    pieces = x.reshape(*dims[:dim], peers, dims[dim] // peers, *dims[dim + 1 :])
    return jnp.moveaxis(pieces, dim, 0)


def summed_on_arrival(x, axis, dim):
    pieces = cut_along(x, dim, lax.axis_size(axis))
    arrived = lax.all_to_all(pieces, axis, split_axis=0, concat_axis=0, tiled=True)
    return arrived.astype(jnp.float32).sum(axis=0)


def from_everyone(x, axis):
    copies = jnp.broadcast_to(x, (lax.axis_size(axis), *x.shape))
    return lax.all_to_all(copies, axis, split_axis=0, concat_axis=0, tiled=True)


def laid_out(pieces, dim):
    pieces = jnp.moveaxis(pieces, 0, dim)
    dims = pieces.shape
    return pieces.reshape(*dims[:dim], dims[dim] * dims[dim + 1], *dims[dim + 2 :])


def collect(x, axis, dim):
    pieces = from_everyone(x, axis)
    return laid_out(pieces, dim)


def in_one_piece(arrays, axis, dim, along):
    widths = [a.shape[along] for a in arrays]
    both = jnp.concatenate(arrays, axis=along)
    result = summed_on_arrival(both, axis, dim)
    return tuple(jnp.split(result, [sum(widths[:k]) for k in range(1, len(widths))], axis=along))


def rms_scale(inputs, scales):
    floats = inputs.astype(jnp.float32)
    return floats * lax.rsqrt(jnp.mean(floats * floats, -1, keepdims=True) + norm_eps) * scales


def slot_ranks(chosen, experts):
    flat_ids = chosen.reshape(-1)
    onehot = (flat_ids[:, None] == jnp.arange(experts, dtype=jnp.int32)[None, :]).astype(jnp.int32)
    earlier = jnp.cumsum(onehot, 0) - onehot
    return jnp.sum(earlier * onehot, 1).reshape(chosen.shape)


def per_device(
    hidden_in,
    mix_gain,
    w_query,
    w_key,
    w_value,
    w_outgate,
    w_gates,
    gate_bias,
    state_matrix,
    state_norm,
    state_max,
    w_mix_out,
    ffn_gain,
    routes,
    route_weights,
    expert_gate,
    expert_up,
    expert_down,
    shared_gate,
    shared_up,
    shared_down,
):
    ep_count = lax.axis_size("ep")
    tp_count = lax.axis_size("tp")
    group_index = lax.axis_index("ep")
    column_index = lax.axis_index("tp")
    seq_rows, width = hidden_in.shape
    heads_dev = state_matrix.shape[1]
    head_dim = state_matrix.shape[2]
    top_count = routes.shape[1]
    local_experts = expert_gate.shape[0]
    expert_total = local_experts * ep_count
    capacity = max(2, seq_rows * top_count // expert_total + 1)
    slot_count = ep_count * capacity
    slice_width = width // tp_count
    normed = rms_scale(hidden_in, mix_gain).astype(jnp.bfloat16)
    gathered = lax.all_to_all(normed, "ep", split_axis=1, concat_axis=0, tiled=True)
    joined = jnp.concatenate([w_query, w_key, w_value, w_outgate], 1)
    projected = summed_on_arrival(
        jnp.dot(gathered, joined, preferred_element_type=jnp.float32).astype(jnp.bfloat16), "ep", 0
    ).astype(jnp.bfloat16)
    head_cols = heads_dev * head_dim

    def heads_of(role_index):
        part = projected[:, role_index * head_cols : (role_index + 1) * head_cols]
        return part.astype(jnp.float32).reshape(seq_rows, heads_dev, head_dim)

    query_heads = heads_of(0)
    key_heads = heads_of(1) * head_dim ** (-0.5)
    value_heads = heads_of(2)
    out_gate = heads_of(3)
    gate_pre = jnp.einsum("sd,gdh->gsh", normed, w_gates, preferred_element_type=jnp.float32)
    gate_pre = gate_pre + gate_bias[:, None, :]
    carried = jax.nn.log_sigmoid(gate_pre[1]) + state_max
    new_max = jnp.maximum(carried, gate_pre[0])
    forget_weight = jnp.exp(carried - new_max)[..., None]
    input_weight = jnp.exp(gate_pre[0] - new_max)[..., None]
    new_norm = forget_weight * state_norm + input_weight * key_heads
    new_matrix = (
        forget_weight[..., None] * state_matrix
        + (input_weight * value_heads)[..., :, None] * key_heads[..., None, :]
    )
    numerator = jnp.einsum("shek,shk->she", new_matrix, query_heads)
    denominator = jnp.maximum(jnp.abs(jnp.sum(new_norm * query_heads, -1)), 1.0)
    gated_out = (jax.nn.sigmoid(out_gate) * numerator / denominator[..., None]).reshape(
        seq_rows, head_cols
    )
    gated_out = gated_out.astype(jnp.bfloat16)
    mixed_part = jnp.dot(gated_out, w_mix_out, preferred_element_type=jnp.float32)
    mixed_own = summed_on_arrival(mixed_part.astype(jnp.bfloat16), "tp", 1)
    residual_own = lax.dynamic_slice_in_dim(hidden_in, column_index * slice_width, slice_width, 1)
    stream_own = (residual_own.astype(jnp.float32) + mixed_own).astype(jnp.bfloat16)
    stream = collect(stream_own, "tp", 1)
    ffn_in = rms_scale(stream, ffn_gain).astype(jnp.bfloat16)
    shared_hidden = (
        jax.nn.silu(jnp.dot(ffn_in, shared_gate, preferred_element_type=jnp.float32))
        * jnp.dot(ffn_in, shared_up, preferred_element_type=jnp.float32)
    ).astype(jnp.bfloat16)
    shared_part = jnp.dot(shared_hidden, shared_down, preferred_element_type=jnp.float32)
    own_routes = lax.dynamic_slice_in_dim(routes, group_index * seq_rows, seq_rows, 0)
    slot_ids = own_routes * capacity + slot_ranks(own_routes, expert_total)
    slot_range = jnp.arange(expert_total * capacity, dtype=jnp.int32)
    matches = slot_ids[:, :, None] == slot_range[None, None, :]
    chooser = jnp.any(matches, 1).astype(jnp.bfloat16)
    outgoing = jnp.einsum("sj,sd->jd", chooser, ffn_in, preferred_element_type=jnp.float32)
    outgoing = outgoing.astype(jnp.bfloat16).reshape(expert_total, capacity, width)
    arrived = lax.all_to_all(outgoing, "ep", split_axis=0, concat_axis=1, tiled=True)
    gate_values = jnp.einsum(
        "erd,edf->erf", arrived, expert_gate, preferred_element_type=jnp.float32
    )
    up_values = jnp.einsum("erd,edf->erf", arrived, expert_up, preferred_element_type=jnp.float32)
    expert_hidden = (jax.nn.silu(gate_values) * up_values).astype(jnp.bfloat16)
    expert_part = jnp.einsum(
        "erf,efd->erd", expert_hidden, expert_down, preferred_element_type=jnp.float32
    )
    expert_part = expert_part.reshape(local_experts * slot_count, width)
    routed_sum, shared_sum = in_one_piece(
        (expert_part.astype(jnp.bfloat16), shared_part.astype(jnp.bfloat16)), "tp", 1, 0
    )
    expert_rows = routed_sum.astype(jnp.bfloat16)
    returned = lax.all_to_all(
        expert_rows.reshape(local_experts, slot_count, slice_width),
        "ep",
        split_axis=1,
        concat_axis=0,
        tiled=True,
    )
    returned = returned.reshape(expert_total * capacity, slice_width)
    weights = jnp.sum(jnp.where(matches, route_weights[:, :, None], 0.0), 1)
    routed = jnp.dot(weights, returned.astype(jnp.float32))
    result = (stream_own.astype(jnp.float32) + shared_sum + routed).astype(jnp.bfloat16)
    return (result, new_matrix, new_norm, new_max)


def solution(mesh):
    placed = (
        P("ep", None),
        P(),
        P("ep", "tp"),
        P("ep", "tp"),
        P("ep", "tp"),
        P("ep", "tp"),
        P(None, None, "tp"),
        P(None, "tp"),
        P("ep", "tp", None, None),
        P("ep", "tp", None),
        P("ep", "tp"),
        P("tp", None),
        P(),
        P(),
        P("ep", None),
        P("ep", None, "tp"),
        P("ep", None, "tp"),
        P("ep", "tp", None),
        P(None, "tp"),
        P(None, "tp"),
        P("tp", None),
    )
    return jax.shard_map(
        per_device,
        mesh=mesh,
        in_specs=placed,
        out_specs=(P("ep", "tp"), P("ep", "tp", None, None), P("ep", "tp", None), P("ep", "tp")),
        check_vma=False,
    )
```

profile of v0, /device:TPU:1, one launch (start us, length us, event | category | flops | bytes accessed | tf_op | source)
XLA Modules:
  0.0 163.9 jit_solution(18080325367607430415)
XLA Ops:
  0.6 1.3 fusion.8
  1.9 1.1 fusion.10
  3.1 14.9 %all_to_all.72 = bf16[32,16,256]{2,0,1:T(8,128)(2,1)S(1)} all-to-all(bf16[32,16,256]{2,0,1:T(8,128)(2,1)S(1)} %bitcast.78), channel_id=1, replica_groups=mesh['ep'=16,'tp'=16] {'ep'}, dimensions={1} | all-to-all | bytes 524288 | tf_op jit(solution)/shard_map/all_to_all | solution.py:93
  18.0 2.0 %convolution_convert_fusion.4 = bf16[512,512]{1,0:T(8,128)(2,1)} fusion(bf16[512,256]{1,0:T(8,128)(2,1)S(1)} %bitcast.79, bf16[256,128]{1,0:T(8,128)(2,1)} %param.26, bf16[256,128]{1,0:T(8,128)(2,1)} %param.25, bf16[256,128]{1,0:T(8,128)(2,1)} %param.24, bf16[256,128]{1,0:T(8,128)(2,1)} %param.23), kind=kOutput, calls=%fused_computation.6 | convolution fusion | flops 135528448 | bytes 1048576 | tf_op jit(solution)/shard_map/dot_general | solution.py:96
  20.0 3.6 %all-to-all-start.1 = ((bf16[16,32,512]{2,1,0:T(8,128)(2,1)}), bf16[16,32,512]{2,1,0:T(8,128)(2,1)S(1)}, u32[]{:S(2)}, u32[]{:S(2)}) async-start(bf16[16,32,512]{2,1,0:T(8,128)(2,1)} %bitcast.3), calls=%async_computation.1 | async-start | bytes 1048576 | tf_op jit(solution)/shard_map/all_to_all | solution.py:17
  23.6 0.2 fusion.3
  24.1 9.0 %all-to-all-done.1 = bf16[16,32,512]{2,1,0:T(8,128)(2,1)S(1)} async-done(((bf16[16,32,512]{2,1,0:T(8,128)(2,1)}), bf16[16,32,512]{2,1,0:T(8,128)(2,1)S(1)}, u32[]{:S(2)}, u32[]{:S(2)}) %all-to-all-start.1) | async-done | bytes 524320 | tf_op jit(solution)/shard_map/all_to_all | solution.py:17
  33.6 0.8 multiply_reduce_fusion
  34.5 2.0 %multiply_add_fusion = f32[32,2,64,64]{3,2,1,0:T(8,128)S(1)} fusion(f32[32,2,64,64]{3,2,1,0:T(8,128)} %param.29, f32[32,2,64]{2,1,0:T(2,128)S(1)} %get-tuple-element.10, f32[32,2,64]{2,1,0:T(2,128)S(1)} %get-tuple-element.14, f32[32,2]{1,0:T(8,128)S(1)} %copy.86), kind=kLoop, calls=%fused_computation.5 | loop fusion | flops 786432 | bytes 2130176 | tf_op jit(solution)/shard_map/add | solution.py:116
  36.5 1.3 copy-done.1
  37.9 0.6 fusion.45
  38.5 0.1 fusion.27
  38.7 0.4 copy-done.4
  39.1 0.3 convolution_convert_fusion.3
  39.3 0.7 copy.115
  40.1 11.6 %all-to-all-start.2 = ((bf16[16,32,256]{2,1,0:T(8,128)(2,1)}), bf16[16,32,256]{2,1,0:T(8,128)(2,1)S(1)}, u32[]{:S(2)}, u32[]{:S(2)}) async-start(bf16[16,32,256]{2,1,0:T(8,128)(2,1)} %bitcast.68), calls=%async_computation.2 | async-start | bytes 524288 | tf_op jit(solution)/shard_map/all_to_all | solution.py:17
  51.6 0.7 constant_dynamic-slice_fusion
  52.5 0.1 eq.28
  52.6 10.6 %all-to-all-done.2 = bf16[16,32,256]{2,1,0:T(8,128)(2,1)S(1)} async-done(((bf16[16,32,256]{2,1,0:T(8,128)(2,1)}), bf16[16,32,256]{2,1,0:T(8,128)(2,1)S(1)}, u32[]{:S(2)}, u32[]{:S(2)}) %all-to-all-start.2) | async-done | bytes 262176 | tf_op jit(solution)/shard_map/all_to_all | solution.py:17
  63.3 0.7 add_convert_fusion
  64.0 0.7 broadcast_in_dim.10
  64.7 3.4 %all-to-all-start.3 = ((bf16[16,32,256]{2,1,0:T(8,128)(2,1)}), bf16[16,32,256]{2,1,0:T(8,128)(2,1)S(1)}, u32[]{:S(2)}, u32[]{:S(2)}) async-start(bf16[16,32,256]{2,1,0:T(8,128)(2,1)} %broadcast_in_dim.10), calls=%async_computation.3 | async-start | bytes 524288 | tf_op jit(solution)/shard_map/all_to_all | solution.py:23
  68.2 0.1 reduce_window_sum.11
  68.3 0.2 select_reduce_fusion.1
  68.5 0.1 reshape.113
  68.8 10.5 %all-to-all-done.3 = bf16[16,32,256]{2,1,0:T(8,128)(2,1)S(1)} async-done(((bf16[16,32,256]{2,1,0:T(8,128)(2,1)}), bf16[16,32,256]{2,1,0:T(8,128)(2,1)S(1)}, u32[]{:S(2)}, u32[]{:S(2)}) %all-to-all-start.3) | async-done | bytes 262176 | tf_op jit(solution)/shard_map/all_to_all | solution.py:23
  79.4 0.2 fusion.11
  79.6 0.1 multiply_convert_fusion
  79.7 0.4 convolution_convert_fusion.1
  80.1 1.3 reshape.114
  81.4 3.7 %all-to-all-start.4 = ((bf16[32,3,4096]{2,1,0:T(4,128)(2,1)}), bf16[32,3,4096]{2,1,0:T(4,128)(2,1)S(1)}, u32[]{:S(2)}, u32[]{:S(2)}) async-start(bf16[32,3,4096]{2,1,0:T(4,128)(2,1)} %reshape.114), calls=%async_computation.4 | async-start | bytes 2097152 | tf_op jit(solution)/shard_map/all_to_all | solution.py:143
  85.1 1.3 fusion.46
  86.4 2.5 %convolution_convert_fusion.2 = bf16[32,4096]{1,0:T(8,128)(2,1)} fusion(bf16[64,4096]{1,0:T(8,128)(2,1)} %param.41, bf16[32,4096]{1,0:T(8,128)(2,1)S(1)} %multiply_convert_fusion, bf16[4096,64]{0,1:T(8,128)(2,1)} %param.40, f32[32,64]{1,0:T(8,128)S(1)} %fusion.46), kind=kOutput, calls=%fused_computation.2 | convolution fusion | flops 33697792 | bytes 1581056 | tf_op jit(solution)/shard_map/dot_general | solution.py:135
  88.9 2.3 %copy.98 = bf16[32,4096]{0,1:T(8,128)(2,1)} copy(bf16[32,4096]{1,0:T(8,128)(2,1)} %convolution_convert_fusion.2) | data formatting | bytes 524288 | tf_op jit(solution)/shard_map/convert_element_type | solution.py:154
  91.2 13.1 %all-to-all-done.4 = bf16[32,3,4096]{2,1,0:T(4,128)(2,1)S(1)} async-done(((bf16[32,3,4096]{2,1,0:T(4,128)(2,1)}), bf16[32,3,4096]{2,1,0:T(4,128)(2,1)S(1)}, u32[]{:S(2)}, u32[]{:S(2)}) %all-to-all-start.4) | async-done | bytes 786464 | tf_op jit(solution)/shard_map/all_to_all | solution.py:143
  104.3 1.0 copy-done.3
  105.3 2.2 %copy.94 = bf16[16,2,3,4096]{3,1,2,0:T(2,128)(2,1)S(1)} copy(bf16[16,2,3,4096]{3,2,1,0:T(4,128)(2,1)} %bitcast.73) | data formatting | bytes 1572864 | tf_op jit(solution)/shard_map/all_to_all | solution.py:143
  107.5 2.6 %fusion.6 = f32[2,48,128]{2,1,0:T(8,128)S(1)} fusion(bf16[2,4096,128]{2,1,0:T(8,128)(2,1)} %param.36, bf16[2,48,4096]{2,0,1:T(2,128)(2,1)S(1)} %bitcast.70), kind=kOutput, calls=%fused_computation.17 | convolution fusion | flops 100663296 | bytes 2932736 | tf_op jit(solution)/shard_map/erd,edf->erf/dot_general | solution.py:144
  110.1 3.9 %convolution_convert_fusion = bf16[2,48,4096]{2,1,0:T(8,128)(2,1)} fusion(bf16[2,128,4096]{2,1,0:T(8,128)(2,1)S(1)} %copy-done, bf16[2,4096,128]{2,1,0:T(8,128)(2,1)} %param.37, bf16[2,48,4096]{2,0,1:T(2,128)(2,1)S(1)} %bitcast.71, f32[2,48,128]{2,1,0:T(8,128)S(1)} %fusion.6), kind=kOutput, calls=%fused_computation | convolution fusion | flops 201793536 | bytes 5816320 | tf_op jit(solution)/shard_map/erf,efd->erd/dot_general | solution.py:149
  114.0 2.3 %copy.97 = bf16[96,4096]{0,1:T(8,128)(2,1)} copy(bf16[96,4096]{1,0:T(8,128)(2,1)} %bitcast.74) | data formatting | bytes 1572864 | tf_op jit(solution)/shard_map/convert_element_type | solution.py:154
  116.3 2.8 %pad_maximum_fusion = bf16[128,4096]{0,1:T(8,128)(2,1)} fusion(bf16[32,4096]{0,1:T(8,128)(2,1)S(1)} %copy-done.2, bf16[96,4096]{0,1:T(8,128)(2,1)} %copy.97), kind=kLoop, calls=%fused_computation.15 | loop fusion | flops 2097152 | bytes 2097152 | tf_op jit(solution)/shard_map/concatenate | solution.py:39
  119.1 1.5 copy.99
  120.6 31.8 %all_to_all.73 = bf16[16,128,256]{2,1,0:T(8,128)(2,1)S(1)} all-to-all(bf16[16,128,256]{2,1,0:T(8,128)(2,1)S(1)} %copy.99), channel_id=1, replica_groups=mesh['ep'=16,'tp'=16] {'tp'}, dimensions={0} | all-to-all | bytes 2097152 | tf_op jit(solution)/shard_map/all_to_all | solution.py:17
  152.4 0.1 convert_reduce_fusion
  152.6 0.7 copy.100
  153.2 3.5 %all-to-all-start.6 = ((bf16[2,48,256]{2,0,1:T(2,128)(2,1)}), bf16[2,48,256]{2,0,1:T(2,128)(2,1)S(1)}, u32[]{:S(2)}, u32[]{:S(2)}) async-start(bf16[2,48,256]{2,0,1:T(2,128)(2,1)} %copy.100), calls=%async_computation.6 | async-start | bytes 98304 | tf_op jit(solution)/shard_map/all_to_all | solution.py:157
  156.8 6.3 %all-to-all-done.6 = bf16[2,48,256]{2,0,1:T(2,128)(2,1)S(1)} async-done(((bf16[2,48,256]{2,0,1:T(2,128)(2,1)}), bf16[2,48,256]{2,0,1:T(2,128)(2,1)S(1)}, u32[]{:S(2)}, u32[]{:S(2)}) %all-to-all-start.6) | async-done | bytes 49184 | tf_op jit(solution)/shard_map/all_to_all | solution.py:157
  163.2 0.7 fusion.1
  (51 shorter events, 1.6 us)
Async XLA Ops:
  0.6 109.5 %copy-start = (bf16[2,128,4096]{2,1,0:T(8,128)(2,1)S(1)}, bf16[2,128,4096]{2,1,0:T(8,128)(2,1)}, u32[]{:S(2)}) copy-start(bf16[2,128,4096]{2,1,0:T(8,128)(2,1)} %param.38) | copy-start | bytes 6291460
  1.9 21.7 %copy-start.10 = (bf16[2,4096,2]{1,2,0:T(2,128)(2,1)S(1)}, bf16[2,4096,2]{1,2,0:T(2,128)(2,1)}, u32[]{:S(2)}) copy-start(bf16[2,4096,2]{1,2,0:T(2,128)(2,1)} %param.27) | copy-start | bytes 98308
  1.9 21.7 %copy-start.11 = (f32[2,2]{1,0:T(2,128)S(1)}, f32[2,2]{1,0:T(2,128)}, u32[]{:S(2)}) copy-start(f32[2,2]{1,0:T(2,128)} %param.28) | copy-start | bytes 52
  3.0 20.8 %copy-start.8 = (f32[32,2]{0,1:T(2,128)S(1)}, f32[32,2]{0,1:T(2,128)}, u32[]{:S(2)}) copy-start(f32[32,2]{0,1:T(2,128)} %param.31) | copy-start | bytes 772
  3.1 30.5 %copy-start.5 = (f32[32,2,64]{2,1,0:T(2,128)S(1)}, f32[32,2,64]{2,1,0:T(2,128)}, u32[]{:S(2)}) copy-start(f32[32,2,64]{2,1,0:T(2,128)} %param.30) | copy-start | bytes 49156
  20.0 13.1 %all-to-all-start.1 = ((bf16[16,32,512]{2,1,0:T(8,128)(2,1)}), bf16[16,32,512]{2,1,0:T(8,128)(2,1)S(1)}, u32[]{:S(2)}, u32[]{:S(2)}) async-start(bf16[16,32,512]{2,1,0:T(8,128)(2,1)} %bitcast.3), calls=%async_computation.1 | async-start | bytes 1048576 | tf_op jit(solution)/shard_map/all_to_all | solution.py:17
  23.8 12.7 %copy-start.7 = (f32[32,2]{0,1:T(2,128)}, f32[32,2]{0,1:T(2,128)S(1)}, u32[]{:S(2)}) copy-start(f32[32,2]{0,1:T(2,128)S(1)} %get-tuple-element.8) | copy-start | bytes 772
  36.5 1.3 copy-start.1
  37.8 1.2 copy-start.4
  40.1 39.5 %copy-start.6 = (f32[4096]{0:T(1024)S(1)}, f32[4096]{0:T(1024)}, u32[]{:S(2)}) copy-start(f32[4096]{0:T(1024)} %param.33) | copy-start | bytes 49156
  40.1 23.2 %all-to-all-start.2 = ((bf16[16,32,256]{2,1,0:T(8,128)(2,1)}), bf16[16,32,256]{2,1,0:T(8,128)(2,1)S(1)}, u32[]{:S(2)}, u32[]{:S(2)}) async-start(bf16[16,32,256]{2,1,0:T(8,128)(2,1)} %bitcast.68), calls=%async_computation.2 | async-start | bytes 524288 | tf_op jit(solution)/shard_map/all_to_all | solution.py:17
  64.7 14.6 %all-to-all-start.3 = ((bf16[16,32,256]{2,1,0:T(8,128)(2,1)}), bf16[16,32,256]{2,1,0:T(8,128)(2,1)S(1)}, u32[]{:S(2)}, u32[]{:S(2)}) async-start(bf16[16,32,256]{2,1,0:T(8,128)(2,1)} %broadcast_in_dim.10), calls=%async_computation.3 | async-start | bytes 524288 | tf_op jit(solution)/shard_map/all_to_all | solution.py:23
  81.4 22.8 %all-to-all-start.4 = ((bf16[32,3,4096]{2,1,0:T(4,128)(2,1)}), bf16[32,3,4096]{2,1,0:T(4,128)(2,1)S(1)}, u32[]{:S(2)}, u32[]{:S(2)}) async-start(bf16[32,3,4096]{2,1,0:T(4,128)(2,1)} %reshape.114), calls=%async_computation.4 | async-start | bytes 2097152 | tf_op jit(solution)/shard_map/all_to_all | solution.py:143
  104.3 1.0 copy-start.3
  114.0 2.3 %copy-start.2 = (bf16[32,4096]{0,1:T(8,128)(2,1)S(1)}, bf16[32,4096]{0,1:T(8,128)(2,1)}, u32[]{:S(2)}) copy-start(bf16[32,4096]{0,1:T(8,128)(2,1)} %copy.98) | copy-start | bytes 786436
  120.6 36.1 %copy-start.9 = (f32[32,2]{0,1:T(2,128)S(1)}, f32[32,2]{0,1:T(2,128)}, u32[]{:S(2)}) copy-start(f32[32,2]{0,1:T(2,128)} %param.35) | copy-start | bytes 772
  153.2 9.9 %all-to-all-start.6 = ((bf16[2,48,256]{2,0,1:T(2,128)(2,1)}), bf16[2,48,256]{2,0,1:T(2,128)(2,1)S(1)}, u32[]{:S(2)}, u32[]{:S(2)}) async-start(bf16[2,48,256]{2,0,1:T(2,128)(2,1)} %copy.100), calls=%async_computation.6 | async-start | bytes 98304 | tf_op jit(solution)/shard_map/all_to_all | solution.py:157
where the time goes:
time: 165 us; the launch traced here: 164 us
  waiting for transfers between devices  49.5 us (30%)
  blocking collectives  46.7 us (28%)
  starting transfers between devices  25.7 us (16%)
  local copies, waits for them, and re-layouts  16.5 us (10%)
  matrix products  14.5 us (9%)
  other arithmetic  9.99 us (6%)
    all_to_all x1, blocking collectives, summed_on_arrival(): lax.all_to_all(pieces, axis, split_axis=0, concat_axis=0, tiled=True)  31.8 us
    all_to_all x2, waiting for transfers between devices, summed_on_arrival(): lax.all_to_all(pieces, axis, split_axis=0, concat_axis=0, tiled=True)  19.6 us
    all_to_all x2, starting transfers between devices, summed_on_arrival(): lax.all_to_all(pieces, axis, split_axis=0, concat_axis=0, tiled=True)  15.1 us
    all_to_all x1, blocking collectives, per_device(): lax.all_to_all(normed, 'ep', split_axis=1, concat_axis=0, tiled=True)  14.9 us
    all_to_all x1, waiting for transfers between devices, per_device(): lax.all_to_all(outgoing, 'ep', split_axis=0, concat_axis=1, tiled=True)  13.1 us
    all_to_all x1, waiting for transfers between devices, from_everyone(): return lax.all_to_all(copies, axis, split_axis=0, concat_axis=0, tiled=True)  10.5 us
    all_to_all x1, waiting for transfers between devices, per_device(): lax.all_to_all(expert_rows.reshape(local_experts, slot_count, slice_width...  6.3 us
    dot_general x1, matrix products, per_device(): jnp.einsum('erf,efd->erd', expert_hidden, expert_down, preferred_element_...  3.86 us
  transfers between devices with their start and end apart: 5, of which 5 were waited for; matrix products, arithmetic and copies ran while one was open for 5% of the time, Pallas kernels for 0%

commit v1 on v0

v1 whole, which is shorter than its diff:
```python
import functools

import jax
import jax.numpy as jnp
from jax import lax
from jax.experimental import pallas as pl
from jax.experimental.pallas import tpu as pltpu
from jax.sharding import PartitionSpec as P

MESH = pl.DeviceIdType.MESH
NORM_EPS = 1e-06
ROOM = 4


def remote(src, dst, send_sem, recv_sem, dev):
    return pltpu.make_async_remote_copy(
        src_ref=src, dst_ref=dst, send_sem=send_sem, recv_sem=recv_sem, device_id=dev, device_id_type=MESH
    )


def wait_bytes(ref, sem):
    pltpu.make_async_copy(ref, ref, sem).wait()


def far_first(n):
    return sorted(range(1, n), key=lambda i: (-min(i, n - i), i))


def near_first(n):
    return sorted(range(1, n), key=lambda i: (min(i, n - i), i))


def layer_kernel(
    cfg,
    hidden_h, mgain_h, wq_h, wk_h, wv_h, wo_h, wg_h, bias_s, state_h, snorm_h, smax_h, wmix_h, fgain_h,
    routes_h, rw_h, eg_h, eu_h, ed_h, sg_h, su_h, sd_h,
    result_o, newmat_o, newnorm_o, newmax_o,
    hid, mgain, wqkvo, wg, state, snorm, smax, wmix, fgain, routes, rw, wcat, down, sgu, sdown,
    xn, ga, pt, qa, kvq, nums, gated, mixs, mixr, mixo, rz, so, st, disp, dx, xg, acc, po, pi, ret, rt, shs, shr, sho, fin, fz,
    nnew, mnew, lsem, s1, r1, s2, r2, s3, r3, s4, r4, s5, r5, s6, r6, s7, r7, s8, r8, s9, r9, s10, r10, s11, r11, s12, r12, osem,
):
    EY, EX, Z, S, D, HD, L = cfg
    E, T = EY * EX, 2 * Z
    W = D // T
    f32, bf16 = jnp.float32, jnp.bfloat16
    e, t = lax.axis_index("ep"), lax.axis_index("tp")
    z, c = lax.div(t, 2), lax.rem(t, 2)
    o = 1 - c
    sib = (e, z * 2 + o)
    y, x = lax.div(e, EX), lax.rem(e, EX)

    def ep_peer(i):
        return lax.rem(y + lax.div(i, EX), EY) * EX + lax.rem(x + lax.rem(i, EX), EX)

    def ep_src(i):
        return lax.rem(y + EY - lax.div(i, EX), EY) * EX + lax.rem(x + EX - lax.rem(i, EX), EX)

    def z_dev(zz):
        return (e, zz * 2 + c)

    def zp(i):
        return lax.rem(z + i, Z)

    def zs(i):
        return lax.rem(z + Z - i, Z)

    def col(zz, cc):
        return pl.ds(pl.multiple_of((zz * 2 + cc) * W, W), W)

    def half(zz):
        return pl.ds(pl.multiple_of(zz * W, W), W)

    def rows(g):
        return pl.ds(pl.multiple_of(g * L * ROOM, L * ROOM), L * ROOM)

    loads = []

    def load(src, dst):
        cp = pltpu.make_async_copy(src, dst, lsem.at[len(loads)])
        cp.start()
        loads.append(cp)
        return cp

    ld_hid = load(hidden_h, hid)
    ld_mg = load(mgain_h, mgain)
    ld_w = [load(w, wqkvo.at[:, k * 128 : (k + 1) * 128]) for k, w in enumerate((wq_h, wk_h, wv_h, wo_h))]
    ld_wg = load(wg_h, wg)
    ld_sm = load(smax_h, smax)
    ld_rt = load(routes_h, routes)
    ld_rw = load(rw_h, rw)
    ld_sn = load(snorm_h, snorm)
    ld_st = load(state_h, state)
    ld_mix = load(wmix_h, wmix)
    ld_fg = load(fgain_h, fgain)
    ld_sg = load(sg_h, sgu.at[0 : sg_h.shape[0], :])
    ld_su = load(su_h, sgu.at[sg_h.shape[0] :, :])
    ld_sd = load(sd_h, sdown)
    ld_ed = load(ed_h, down)
    cat_sem = lsem.at[len(loads)]

    def cat_copies(k):
        zz, cc = lax.div(k, 2), lax.rem(k, 2)
        return [
            pltpu.make_async_copy(
                src.at[j, pl.ds(pl.multiple_of(k * W, W), W), :],
                wcat.at[cc, pl.ds(pl.multiple_of(zz * W, W), W), (2 * j + q) * 128 : (2 * j + q + 1) * 128],
                cat_sem,
            )
            for j in range(L)
            for q, src in enumerate((eg_h, eu_h))
        ]

    def start_cat(k, _):
        for cp in cat_copies(k):
            cp.start()
        return 0

    lax.fori_loop(0, T, start_cat, 0)

    barrier = pltpu.get_barrier_semaphore()

    def greet(i, _):
        pl.semaphore_signal(barrier, inc=1, device_id=(ep_peer(i), t), device_id_type=MESH)
        return 0

    lax.fori_loop(1, E, greet, 0)
    for i in range(1, Z):
        pl.semaphore_signal(barrier, inc=1, device_id=z_dev(zp(i)), device_id_type=MESH)
    pl.semaphore_signal(barrier, inc=1, device_id=sib, device_id_type=MESH)

    ld_hid.wait()
    ld_mg.wait()
    KS = D // E
    sq = jnp.zeros((S, 128), f32)
    for k in range(D // 128):
        v = hid[:, k * 128 : (k + 1) * 128].astype(f32)
        sq = sq + v * v
    scale = lax.rsqrt(jnp.sum(sq, -1, keepdims=True) * (1.0 / D) + NORM_EPS)
    for k in range(E):
        v = hid[:, k * KS : (k + 1) * KS].astype(f32)
        xn[k] = (v * scale * mgain[:, k * KS : (k + 1) * KS]).astype(bf16)

    pl.semaphore_wait(barrier, E - 1 + Z - 1 + 1)

    def send_x(i, _):
        p = ep_peer(i)
        remote(xn.at[p], ga.at[e], s1.at[i], r1.at[i], (p, t)).start()
        return 0

    lax.fori_loop(1, E, send_x, 0)

    for cp in ld_w:
        cp.wait()
    qa[0] = jnp.dot(xn[e], wqkvo[...], preferred_element_type=f32).astype(bf16)

    ld_wg.wait()
    ld_sm.wait()
    ld_rt.wait()
    ld_rw.wait()
    HN = 2
    gsum = [[jnp.zeros((S, 128), f32) for _ in range(HN)] for _ in range(2)]
    for k in range(D // 128):
        v = xn[k * 128 // KS, :, (k * 128) % KS : (k * 128) % KS + 128].astype(f32)
        for g in range(2):
            w2 = wg[g, :, k * 128 : (k + 1) * 128].astype(f32)
            for h in range(HN):
                gsum[g][h] = gsum[g][h] + v * w2[h : h + 1, :]
    eye = lax.broadcasted_iota(jnp.int32, (S, S), 0) == lax.broadcasted_iota(jnp.int32, (S, S), 1)
    smax_v = smax[...]
    fws, iws = [], []
    for h in range(HN):
        gi = jnp.sum(gsum[0][h], -1, keepdims=True) + bias_s[0, h]
        gf = jnp.sum(gsum[1][h], -1, keepdims=True) + bias_s[1, h]
        old = jnp.sum(jnp.where(eye, smax_v[h : h + 1, :], 0.0), -1, keepdims=True)
        carried = jnp.minimum(gf, 0.0) - jnp.log(1.0 + jnp.exp(-jnp.abs(gf))) + old
        nm = jnp.maximum(carried, gi)
        fws.append(jnp.exp(carried - nm))
        iws.append(jnp.exp(gi - nm))
        mnew[h : h + 1, :] = jnp.sum(jnp.where(eye, nm, 0.0), 0, keepdims=True)

    GR = routes_h.shape[1]
    sel = (
        lax.broadcasted_iota(jnp.int32, (S, GR), 1) == lax.broadcasted_iota(jnp.int32, (S, GR), 0) + e * S
    )
    all_routes = routes[...].astype(f32)
    sel_f = jnp.where(sel, 1.0, 0.0)
    r_col = [jnp.sum(sel_f * all_routes[j : j + 1, :], -1, keepdims=True) for j in range(2)]
    r_row = [jnp.sum(jnp.where(eye, r_col[j], 0.0), 0, keepdims=True) for j in range(2)]
    i0 = lax.broadcasted_iota(jnp.int32, (S, S), 0)
    i1 = lax.broadcasted_iota(jnp.int32, (S, S), 1)
    NS = E * L * ROOM
    slot_row, slot_col = [], []
    for j in range(2):
        same = jnp.where(r_col[0] == r_row[j], 1.0, 0.0) + jnp.where(r_col[1] == r_row[j], 1.0, 0.0)
        rank_row = jnp.sum(jnp.where(i0 < i1, same, 0.0), 0, keepdims=True)
        slot_row.append(r_row[j] * ROOM + rank_row)
        same = jnp.where(r_row[0] == r_col[j], 1.0, 0.0) + jnp.where(r_row[1] == r_col[j], 1.0, 0.0)
        rank_col = jnp.sum(jnp.where(i1 < i0, same, 0.0), -1, keepdims=True)
        slot_col.append(r_col[j] * ROOM + rank_col)
    slot_ids = lax.broadcasted_iota(jnp.int32, (NS, S), 0).astype(f32)
    chooser = jnp.where((slot_ids == slot_row[0]) | (slot_ids == slot_row[1]), 1.0, 0.0).astype(bf16)
    rw_v = rw[...]
    rw_col = [jnp.sum(jnp.where(eye, rw_v[j : j + 1, :], 0.0), -1, keepdims=True) for j in range(2)]
    lane_ids = lax.broadcasted_iota(jnp.int32, (S, NS), 1).astype(f32)
    wsel = jnp.where(lane_ids == slot_col[0], rw_col[0], 0.0) + jnp.where(lane_ids == slot_col[1], rw_col[1], 0.0)
    w_hi = wsel.astype(bf16)
    w_lo = (wsel - w_hi.astype(f32)).astype(bf16)

    def project(i, _):
        g = ep_src(i)
        remote(xn.at[g], ga.at[g], s1.at[i], r1.at[i], (g, t)).wait_recv()
        pt[g] = jnp.dot(ga[g], wqkvo[...], preferred_element_type=f32).astype(bf16)
        remote(pt.at[g], qa.at[i], s2.at[i], r2.at[i], (g, t)).start()
        return 0

    lax.fori_loop(1, E, project, 0)

    ld_sn.wait()
    ld_st.wait()

    def arrived(i, _):
        g = ep_peer(i)
        remote(pt.at[g], qa.at[i], s2.at[i], r2.at[i], (g, t)).wait_recv()
        return 0

    lax.fori_loop(1, E, arrived, 0)
    roles = []
    for k in range(4):
        total = qa[0, :, k * 128 : (k + 1) * 128].astype(f32)
        for i in range(1, E):
            total = total + qa[i, :, k * 128 : (k + 1) * 128].astype(f32)
        roles.append(total.astype(bf16).astype(f32))

    for h in range(HN):
        hs = slice(h * HD, (h + 1) * HD)
        qh, kh, vh = roles[0][:, hs], roles[1][:, hs] * HD ** (-0.5), roles[2][:, hs]
        kvq[h, 0] = qh
        kvq[h, 1] = kh
        kvq[h, 2] = vh * iws[h]
        kvq[h, 3] = jnp.broadcast_to(fws[h], (S, HD))
    SB = 8

    def cell(b, _):
        at = pl.ds(pl.multiple_of(b * SB, SB), SB)
        for h in range(HN):
            new = (
                kvq[h, 3, at, :][:, None, :] * state[at, h]
                + kvq[h, 2, at, :][:, :, None] * kvq[h, 1, at, :][:, None, :]
            )
            state[at, h] = new
            nums[h, at, :] = jnp.sum(new * kvq[h, 0, at, :][:, None, :], -1)
        return 0

    lax.fori_loop(0, S // SB, cell, 0)
    out_mat = pltpu.make_async_copy(state, newmat_o, osem.at[0])
    out_mat.start()
    for h in range(HN):
        hs = slice(h * HD, (h + 1) * HD)
        nn = fws[h] * snorm[:, h, :] + iws[h] * kvq[h, 1]
        nnew[:, h, :] = nn
        den = jnp.maximum(jnp.abs(jnp.sum(nn * kvq[h, 0], -1, keepdims=True)), 1.0)
        gate = 1.0 / (1.0 + jnp.exp(-roles[3][:, hs]))
        gated[:, hs] = (gate * nums[h] / den).astype(bf16)
    out_norm = pltpu.make_async_copy(nnew, newnorm_o, osem.at[1])
    out_norm.start()
    out_max = pltpu.make_async_copy(mnew, newmax_o, osem.at[2])
    out_max.start()

    ld_mix.wait()
    gv = gated[...]
    zorder = far_first(Z) + [0]
    for i in zorder:
        zz = zp(i)
        mixs[zz] = jnp.dot(gv, wmix[:, col(zz, o)], preferred_element_type=f32).astype(bf16)
        remote(mixs.at[zz], mixr.at[zz], s3.at[i], r3.at[i], sib).start()
    own = None
    for i in zorder:
        zz = zp(i)
        mine = jnp.dot(gv, wmix[:, col(zz, c)], preferred_element_type=f32)
        remote(mixs.at[zz], mixr.at[zz], s3.at[i], r3.at[i], sib).wait_recv()
        both = mine + mixr[zz].astype(f32)
        if i:
            mixo[zz] = both.astype(bf16)
            remote(mixo.at[zz], rz.at[i], s4.at[i], r4.at[i], z_dev(zz)).start()
        else:
            own = both
    own = own + hid[:, pl.ds(pl.multiple_of(t * W, W), W)].astype(f32)
    for i in near_first(Z):
        remote(mixo.at[zs(i)], rz.at[i], s4.at[i], r4.at[i], z_dev(zs(i))).wait_recv()
        own = own + rz[i].astype(f32)
    so[...] = own.astype(bf16)

    for i in far_first(Z):
        remote(so, st.at[c, z], s5.at[i], r5.at[i], z_dev(zp(i))).start()
    remote(so, st.at[c, z], s6.at[0], r6.at[0], sib).start()
    st[c, z] = so[...]
    disp[:, half(z)] = jnp.dot(chooser, so[...], preferred_element_type=f32).astype(bf16)
    for i in near_first(Z):
        g = zs(i)
        remote(so, st.at[c, g], s5.at[i], r5.at[i], z_dev(g)).wait_recv()
        remote(st.at[c, g], st.at[c, g], s6.at[i], r6.at[i], sib).start()
        disp[:, half(g)] = jnp.dot(chooser, st[c, g], preferred_element_type=f32).astype(bf16)

    def send_rows(i, _):
        p = ep_peer(i)
        remote(disp.at[rows(p)], dx.at[c, rows(e)], s7.at[i], r7.at[i], (p, t)).start()
        return 0

    lax.fori_loop(1, E, send_rows, 0)
    remote(disp.at[rows(e)], dx.at[c, rows(e)], s8.at[0], r8.at[0], sib).start()
    keep = pltpu.make_async_copy(disp.at[rows(e)], dx.at[c, rows(e)], osem.at[3])
    keep.start()

    ld_fg.wait()
    ld_sg.wait()
    ld_su.wait()
    ld_sd.wait()
    for i in range(Z):
        remote(st.at[c, z], st.at[o, zs(i)], s6.at[i], r6.at[i], sib).wait_recv()
    sq = jnp.zeros((S, W), f32)
    for cc in range(2):
        for zz in range(Z):
            v = st[cc, zz].astype(f32)
            sq = sq + v * v
    sscale = lax.rsqrt(jnp.sum(sq, -1, keepdims=True) * (1.0 / D) + NORM_EPS)
    pre = jnp.zeros((S, sgu.shape[0]), f32)
    for cc in range(2):
        for zz in range(Z):
            cs = slice((zz * 2 + cc) * W, (zz * 2 + cc + 1) * W)
            v = (st[cc, zz].astype(f32) * sscale * fgain[:, cs]).astype(bf16)
            pre = pre + lax.dot_general(v, sgu[:, cs], (((1,), (1,)), ((), ())), preferred_element_type=f32)
    SW = sg_h.shape[0]
    sgate, sup = pre[:, :SW], pre[:, SW:]
    shid = (sgate / (1.0 + jnp.exp(-sgate)) * sup).astype(bf16)
    for zz in range(Z):
        shs[zz] = jnp.dot(shid, sdown[:, col(zz, o)], preferred_element_type=f32).astype(bf16)
    remote(shs, shr, s9.at[0], r9.at[0], sib).start()
    for zz in range(Z):
        sho[zz] = jnp.dot(shid, sdown[:, col(zz, c)], preferred_element_type=f32)

    def pass_on(i, _):
        g = ep_src(i)
        remote(disp.at[rows(g)], dx.at[c, rows(g)], s7.at[i], r7.at[i], (g, t)).wait_recv()
        remote(dx.at[c, rows(g)], dx.at[c, rows(g)], s8.at[i], r8.at[i], sib).start()
        return 0

    lax.fori_loop(1, E, pass_on, 0)
    keep.wait()
    wait_bytes(wcat, cat_sem)

    def prepare(cc, sq):
        def piece(zz, sq):
            v = dx[cc, :, half(zz)].astype(f32)
            xg[cc, :, half(zz)] = (v * fgain[:, col(zz, cc)]).astype(bf16)
            v = v * v
            for k in range(W // 128):
                sq = sq + v[:, k * 128 : (k + 1) * 128]
            return sq

        return lax.fori_loop(0, Z, piece, sq)

    sq = prepare(c, jnp.zeros((NS, 128), f32))
    acc[...] = jnp.dot(xg[c], wcat[c], preferred_element_type=f32)

    def from_sibling(i, _):
        g = ep_src(i)
        remote(dx.at[c, rows(g)], dx.at[o, rows(g)], s8.at[i], r8.at[i], sib).wait_recv()
        return 0

    lax.fori_loop(0, E, from_sibling, 0)
    sq = prepare(o, sq)
    acc[...] += jnp.dot(xg[o], wcat[o], preferred_element_type=f32)
    escale = lax.rsqrt(jnp.sum(sq, -1, keepdims=True) * (1.0 / D) + NORM_EPS)
    expert_of = lax.rem(lax.div(lax.broadcasted_iota(jnp.int32, (NS, 128), 0), ROOM), L)
    hids = []
    for j in range(L):
        gv = acc[:, 2 * j * 128 : (2 * j + 1) * 128] * escale
        uv = acc[:, (2 * j + 1) * 128 : (2 * j + 2) * 128] * escale
        hids.append(jnp.where(expert_of == j, gv / (1.0 + jnp.exp(-gv)) * uv, 0.0).astype(bf16))
    hcat = jnp.concatenate(hids, 1)

    ld_ed.wait()

    def down_of(zz, cc):
        total = None
        for j in range(1):
            w = down[:, :, col(zz, cc)].reshape(L * 128, W)
            total = jnp.dot(hcat, w, preferred_element_type=f32)
        return total

    for zz in range(Z):
        po[zz] = down_of(zz, o).astype(bf16)
        remote(po.at[zz], pi.at[zz], s10.at[zz], r10.at[zz], sib).start()
    for zz in range(Z):
        mine = down_of(zz, c)
        remote(po.at[zz], pi.at[zz], s10.at[zz], r10.at[zz], sib).wait_recv()
        ret[:, zz * W : (zz + 1) * W] = (mine + pi[zz].astype(f32)).astype(bf16)

    def send_back(i, _):
        p = ep_peer(i)
        remote(ret.at[rows(p)], rt.at[rows(e)], s11.at[i], r11.at[i], (p, t)).start()
        return 0

    lax.fori_loop(1, E, send_back, 0)
    keep2 = pltpu.make_async_copy(ret.at[rows(e)], rt.at[rows(e)], osem.at[4])
    keep2.start()
    remote(shs, shr, s9.at[0], r9.at[0], sib).wait_recv()
    w_both = jnp.concatenate([w_hi, w_lo], 0)
    keep2.wait()

    def came_back(i, _):
        g = ep_src(i)
        remote(ret.at[rows(g)], rt.at[rows(g)], s11.at[i], r11.at[i], (g, t)).wait_recv()
        return 0

    lax.fori_loop(1, E, came_back, 0)
    own = None
    for i in zorder:
        zz = zp(i)
        two = jnp.dot(w_both, rt[:, half(zz)], preferred_element_type=f32)
        both = two[:S] + two[S:] + sho[zz] + shr[zz].astype(f32)
        if i:
            fin[zz] = both.astype(bf16)
            remote(fin.at[zz], fz.at[i], s12.at[i], r12.at[i], z_dev(zz)).start()
        else:
            own = both
    own = own + so[...].astype(f32)
    for i in near_first(Z):
        remote(fin.at[zs(i)], fz.at[i], s12.at[i], r12.at[i], z_dev(zs(i))).wait_recv()
        own = own + fz[i].astype(f32)
    result_o[...] = own.astype(bf16)

    def drain(i, _):
        p = ep_peer(i)
        remote(xn.at[p], ga.at[e], s1.at[i], r1.at[i], (p, t)).wait_send()
        remote(pt.at[p], qa.at[i], s2.at[i], r2.at[i], (p, t)).wait_send()
        remote(disp.at[rows(p)], dx.at[c, rows(e)], s7.at[i], r7.at[i], (p, t)).wait_send()
        remote(ret.at[rows(p)], rt.at[rows(e)], s11.at[i], r11.at[i], (p, t)).wait_send()
        return 0

    lax.fori_loop(1, E, drain, 0)

    def drain_sib(i, _):
        remote(disp.at[rows(e)], dx.at[c, rows(e)], s8.at[i], r8.at[i], sib).wait_send()
        return 0

    lax.fori_loop(0, E, drain_sib, 0)
    for i in range(Z):
        remote(mixs.at[z], mixr.at[z], s3.at[i], r3.at[i], sib).wait_send()
        remote(so, st.at[c, z], s6.at[i], r6.at[i], sib).wait_send()
        remote(po.at[i], pi.at[i], s10.at[i], r10.at[i], sib).wait_send()
        if i:
            remote(mixo.at[z], rz.at[i], s4.at[i], r4.at[i], z_dev(zp(i))).wait_send()
            remote(so, st.at[c, z], s5.at[i], r5.at[i], z_dev(zp(i))).wait_send()
            remote(fin.at[z], fz.at[i], s12.at[i], r12.at[i], z_dev(zp(i))).wait_send()
    remote(shs, shr, s9.at[0], r9.at[0], sib).wait_send()
    out_mat.wait()
    out_norm.wait()
    out_max.wait()


def per_device(shape, *args):
    (hidden, mgain, wq, wk, wv, wo, wgates, bias, state, snorm, smax, wmix, fgain, routes, rw, eg, eu, ed, sg, su, sd) = args
    E, T = shape["ep"], shape["tp"]
    EX = 4 if E % 4 == 0 and E > 4 else 2
    EY, Z = E // EX, T // 2
    S, D = hidden.shape
    HN, HD = state.shape[1], state.shape[2]
    L, SW = eg.shape[0], sg.shape[1]
    W, KS, NS = D // T, D // E, E * L * ROOM
    f32, bf16 = jnp.float32, jnp.bfloat16
    V, dma = pltpu.VMEM, pltpu.SemaphoreType.DMA
    scratch = [
        V((S, D), bf16), V((1, D), f32), V((KS, 512), bf16), V((2, HN, D), bf16), V(state.shape, f32), V(snorm.shape, f32),
        V((HN, S), f32), V(wmix.shape, bf16), V((1, D), f32), V((2, routes.shape[0]), jnp.int32), V((2, S), f32),
        V((2, D // 2, 4 * 128), bf16), V(ed.shape, bf16), V((2 * SW, D), bf16), V((SW, D), bf16),
        V((E, S, KS), bf16), V((E, S, KS), bf16), V((E, S, 512), bf16), V((E, S, 512), bf16),
        V((HN, 4, S, HD), f32), V((HN, S, HD), f32), V((S, HN * HD), bf16),
        V((Z, S, W), bf16), V((Z, S, W), bf16), V((Z, S, W), bf16), V((Z, S, W), bf16),
        V((S, W), bf16), V((2, Z, S, W), bf16), V((NS, D // 2), bf16), V((2, NS, D // 2), bf16), V((2, NS, D // 2), bf16),
        V((NS, 512), f32), V((Z, NS, W), bf16), V((Z, NS, W), bf16), V((NS, D // 2), bf16), V((NS, D // 2), bf16),
        V((Z, S, W), bf16), V((Z, S, W), bf16), V((Z, S, W), f32), V((Z, S, W), bf16), V((Z, S, W), bf16),
        V(snorm.shape, f32), V((HN, S), f32),
        dma((24,)),
        dma((E,)), dma((E,)), dma((E,)), dma((E,)), dma((Z,)), dma((Z,)), dma((Z,)), dma((Z,)), dma((Z,)), dma((Z,)),
        dma((Z,)), dma((Z,)), dma((E,)), dma((E,)), dma((E,)), dma((E,)), dma((1,)), dma((1,)), dma((Z,)), dma((Z,)),
        dma((E,)), dma((E,)), dma((Z,)), dma((Z,)), dma((5,)),
    ]
    anywhere = pl.BlockSpec(memory_space=pl.ANY)
    hbm = pl.BlockSpec(memory_space=pltpu.HBM)
    in_specs = [hbm] * 21
    in_specs[7] = pl.BlockSpec(memory_space=pltpu.SMEM)
    vm = pl.BlockSpec(memory_space=pltpu.VMEM)
    result, newmat, newnorm, newmax = pl.pallas_call(
        functools.partial(layer_kernel, (EY, EX, Z, S, D, HD, L)),
        out_shape=(
            jax.ShapeDtypeStruct((S, W), bf16),
            jax.ShapeDtypeStruct(state.shape, f32),
            jax.ShapeDtypeStruct(snorm.shape, f32),
            jax.ShapeDtypeStruct((HN, S), f32),
        ),
        in_specs=in_specs,
        out_specs=(vm, anywhere, anywhere, anywhere),
        scratch_shapes=scratch,
        compiler_params=pltpu.CompilerParams(
            collective_id=0, has_side_effects=True, vmem_limit_bytes=48 * 1024 * 1024
        ),
        name="layer",
    )(
        hidden, mgain.reshape(1, D), wq, wk, wv, wo, jnp.swapaxes(wgates, 1, 2), bias, state, snorm, smax.T, wmix,
        fgain.reshape(1, D), routes.T, rw.T, eg, eu, ed, sg.T, su.T, sd,
    )
    return result, newmat, newnorm, newmax.T


def solution(mesh):
    placed = (
        P("ep", None),
        P(),
        P("ep", "tp"),
        P("ep", "tp"),
        P("ep", "tp"),
        P("ep", "tp"),
        P(None, None, "tp"),
        P(None, "tp"),
        P("ep", "tp", None, None),
        P("ep", "tp", None),
        P("ep", "tp"),
        P("tp", None),
        P(),
        P(),
        P("ep", None),
        P("ep", None, "tp"),
        P("ep", None, "tp"),
        P("ep", "tp", None),
        P(None, "tp"),
        P(None, "tp"),
        P("tp", None),
    )
    return jax.shard_map(
        functools.partial(per_device, dict(mesh.shape)),
        mesh=mesh,
        in_specs=placed,
        out_specs=(P("ep", "tp"), P("ep", "tp", None, None), P("ep", "tp", None), P("ep", "tp")),
        check_vma=False,
    )
```

time: 165 us -> 88.3 us (0.54)
  Pallas kernels: 0 us -> 69.4 us
  waiting for transfers between devices: 49.5 us -> 0 us
  blocking collectives: 46.7 us -> 0 us
  starting transfers between devices: 25.7 us -> 0 us
  matrix products: 14.5 us -> 0 us
  other arithmetic: 9.99 us -> 0 us
    pallas_call x0 -> x1, Pallas kernels: none -> 69.4 us  [per_device(): pl.pallas_call(functools.partial(layer_kernel, (EY, EX, Z, S, D, HD, L)),...]
    all_to_all x5 -> x0, waiting for transfers between devices: 49.5 us -> none  [the longest x2 19.6 us: summed_on_arrival(): lax.all_to_all(pieces, axis, split_axis=0, concat_axis=0, tiled=True)]
    all_to_all x2 -> x0, blocking collectives: 46.7 us -> none  [the longest x1 31.8 us: summed_on_arrival(): lax.all_to_all(pieces, axis, split_axis=0, concat_axis=0, tiled=True)]
    all_to_all x5 -> x0, starting transfers between devices: 25.7 us -> none  [the longest x2 15.1 us: summed_on_arrival(): lax.all_to_all(pieces, axis, split_axis=0, concat_axis=0, tiled=True)]
    unnamed x25 -> x38, local copies, waits for them, and re-layouts: 2.86 us -> 17.4 us
    dot_general x10 -> x0, matrix products: 14.5 us -> none  [the longest x1 3.86 us: per_device(): jnp.einsum('erf,efd->erd', expert_hidden, expert_down, preferred_element_...]
    convert_element_type x4 -> x0, local copies, waits for them, and re-layouts: 4.74 us -> none  [the longest x1 2.33 us: per_device(): expert_part.astype(jnp.bfloat16)]
    reshape x9 -> x0, local copies, waits for them, and re-layouts: 3.18 us -> none  [the longest x1 1.31 us: per_device(): outgoing.astype(jnp.bfloat16).reshape(expert_total, capacity, width)]
  transfers between devices with their start and end apart: 5 -> 0, of which waited for: 5 -> 0; matrix products, arithmetic and copies ran while one was open for 5% -> 0% of each run, Pallas kernels for 0% -> 0%
where the time goes in v1:
time: 88.3 us; the launch traced here: 87.5 us
  Pallas kernels  69.4 us (79%)
  local copies, waits for them, and re-layouts  17.4 us (20%)
    pallas_call x1, Pallas kernels, per_device(): pl.pallas_call(functools.partial(layer_kernel, (EY, EX, Z, S, D, HD, L)),...  69.4 us
    unnamed x38, local copies, waits for them, and re-layouts  17.4 us

profile of v1, /device:TPU:1, one launch (start us, length us, event | category | flops | bytes accessed | tf_op | source)
XLA Modules:
  0.0 87.5 jit_solution(1361231350220668165)
XLA Ops:
  0.6 0.0 copy-start
  0.6 1.2 %copy-done = bf16[128,4096]{1,0:T(8,128)(2,1)S(1)} copy-done((bf16[128,4096]{1,0:T(8,128)(2,1)S(1)}, bf16[128,4096]{1,0:T(8,128)(2,1)}, u32[]{:S(2)}) %copy-start) | copy-done | bytes 1048600
  1.9 0.0 copy-start.1
  1.9 1.0 %copy-done.1 = bf16[4096,64]{0,1:T(8,128)(2,1)S(1)} copy-done((bf16[4096,64]{0,1:T(8,128)(2,1)S(1)}, bf16[4096,64]{0,1:T(8,128)(2,1)}, u32[]{:S(2)}) %copy-start.1) | copy-done | bytes 524312
  2.9 0.0 copy-start.2
  2.9 1.0 %copy-done.2 = bf16[4096,64]{0,1:T(8,128)(2,1)S(1)} copy-done((bf16[4096,64]{0,1:T(8,128)(2,1)S(1)}, bf16[4096,64]{0,1:T(8,128)(2,1)}, u32[]{:S(2)}) %copy-start.2) | copy-done | bytes 524312
  3.9 0.0 copy-start.3
  4.0 1.0 %copy-done.3 = bf16[64,4096]{1,0:T(8,128)(2,1)S(1)} copy-done((bf16[64,4096]{1,0:T(8,128)(2,1)S(1)}, bf16[64,4096]{1,0:T(8,128)(2,1)}, u32[]{:S(2)}) %copy-start.3) | copy-done | bytes 524312
  5.0 0.0 copy-start.4
  5.0 0.9 %copy-done.4 = bf16[32,4096]{1,0:T(8,128)(2,1)S(1)} copy-done((bf16[32,4096]{1,0:T(8,128)(2,1)S(1)}, bf16[32,4096]{1,0:T(8,128)(2,1)}, u32[]{:S(2)}) %copy-start.4) | copy-done | bytes 262168
  5.9 0.0 copy-start.5
  5.9 0.8 copy-done.5
  6.8 0.0 copy-start.6
  6.8 0.8 copy-done.6
  7.6 0.0 copy-start.7
  7.6 0.8 copy-done.7
  8.5 0.0 copy-start.8
  8.5 0.8 copy-done.8
  9.3 0.0 copy-start.9
  9.3 0.8 copy-done.9
  10.1 0.0 copy-start.10
  10.1 0.8 copy-done.10
  10.8 0.0 copy-start.11
  10.8 0.7 copy-done.11
  11.5 0.0 copy-start.12
  11.5 0.7 copy-done.12
  12.3 0.0 copy-start.13
  12.3 0.7 copy-done.13
  12.9 0.0 copy-start.14
  12.9 0.7 copy-done.14
  13.6 0.0 copy-start.15
  13.6 0.7 copy-done.15
  14.3 0.0 copy-start.16
  14.3 0.7 copy-done.16
  15.0 69.4 %layer.1 = (bf16[32,256]{1,0:T(8,128)(2,1)S(1)}, f32[32,2,64,64]{3,2,1,0:T(8,128)S(1)}, f32[32,2,64]{2,1,0:T(2,128)S(1)}, f32[2,32]{1,0:T(2,128)S(1)}) custom-call(bf16[32,4096]{1,0:T(8,128)(2,1)S(1)} %copy-done.4, f32[1,4096]{1,0:T(1,128)S(1)} %bitcast.12, bf16[256,128]{1,0:T(8,128)(2,1)S(1)} %copy-done.5, bf16[256,128]{1,0:T(8,128)(2,1)S(1)} %copy-done.6, ...), custom_call_target="tpu_custom_call" | custom-call | tf_op jit(solution)/shard_map/layer/pallas_call | solution.py:494
  84.4 0.6 copy.29
  85.0 1.3 %copy.30 = f32[32,2,64,64]{3,2,1,0:T(8,128)} copy(f32[32,2,64,64]{3,2,1,0:T(8,128)S(1)} %get-tuple-element.17) | data formatting | bytes 2097152
  86.3 0.6 copy.31
  86.9 0.6 copy.32
Async XLA Ops:
  0.6 1.2 %copy-start = (bf16[128,4096]{1,0:T(8,128)(2,1)S(1)}, bf16[128,4096]{1,0:T(8,128)(2,1)}, u32[]{:S(2)}) copy-start(bf16[128,4096]{1,0:T(8,128)(2,1)} %wmix_h.1) | copy-start | bytes 3145732
  1.9 1.0 %copy-start.1 = (bf16[4096,64]{0,1:T(8,128)(2,1)S(1)}, bf16[4096,64]{0,1:T(8,128)(2,1)}, u32[]{:S(2)}) copy-start(bf16[4096,64]{0,1:T(8,128)(2,1)} %param.39) | copy-start | bytes 1572868
  2.9 1.0 %copy-start.2 = (bf16[4096,64]{0,1:T(8,128)(2,1)S(1)}, bf16[4096,64]{0,1:T(8,128)(2,1)}, u32[]{:S(2)}) copy-start(bf16[4096,64]{0,1:T(8,128)(2,1)} %param.40) | copy-start | bytes 1572868
  3.9 1.0 %copy-start.3 = (bf16[64,4096]{1,0:T(8,128)(2,1)S(1)}, bf16[64,4096]{1,0:T(8,128)(2,1)}, u32[]{:S(2)}) copy-start(bf16[64,4096]{1,0:T(8,128)(2,1)} %sd_h.1) | copy-start | bytes 1572868
  5.0 0.9 %copy-start.4 = (bf16[32,4096]{1,0:T(8,128)(2,1)S(1)}, bf16[32,4096]{1,0:T(8,128)(2,1)}, u32[]{:S(2)}) copy-start(bf16[32,4096]{1,0:T(8,128)(2,1)} %hidden_h.1) | copy-start | bytes 786436
  5.9 0.8 copy-start.5
  6.8 0.8 copy-start.6
  7.6 0.8 copy-start.7
  8.5 0.8 copy-start.8
  9.3 0.8 copy-start.9
  10.1 0.8 copy-start.10
  10.8 0.7 copy-start.11
  11.5 0.7 copy-start.12
  12.3 0.7 copy-start.13
  12.9 0.7 copy-start.14
  13.6 0.7 copy-start.15
  14.3 0.7 copy-start.16

commit v2 on v1

--- a/solution.py
+++ b/solution.py
@@ -32,10 +32,10 @@
 
 def layer_kernel(
     cfg,
-    hidden_h, mgain_h, wq_h, wk_h, wv_h, wo_h, wg_h, bias_s, state_h, snorm_h, smax_h, wmix_h, fgain_h,
+    hidden_h, mgain_h, wq_h, wk_h, wv_h, wo_h, wg_h, bias_h, state_h, snorm_h, smax_h, wmix_h, fgain_h,
     routes_h, rw_h, eg_h, eu_h, ed_h, sg_h, su_h, sd_h,
     result_o, newmat_o, newnorm_o, newmax_o,
-    hid, mgain, wqkvo, wg, state, snorm, smax, wmix, fgain, routes, rw, wcat, down, sgu, sdown,
+    hid, mgain, wqkvo, wg, bias, state, snorm, smax, wmix, fgain, routes, rw, wcat, down, sgu, sdown,
     xn, ga, pt, qa, kvq, nums, gated, mixs, mixr, mixo, rz, so, st, disp, dx, xg, acc, po, pi, ret, rt, shs, shr, sho, fin, fz,
     nnew, mnew, lsem, s1, r1, s2, r2, s3, r3, s4, r4, s5, r5, s6, r6, s7, r7, s8, r8, s9, r9, s10, r10, s11, r11, s12, r12, osem,
 ):
@@ -85,6 +85,7 @@
     ld_mg = load(mgain_h, mgain)
     ld_w = [load(w, wqkvo.at[:, k * 128 : (k + 1) * 128]) for k, w in enumerate((wq_h, wk_h, wv_h, wo_h))]
     ld_wg = load(wg_h, wg)
+    ld_bi = load(bias_h, bias)
     ld_sm = load(smax_h, smax)
     ld_rt = load(routes_h, routes)
     ld_rw = load(rw_h, rw)
@@ -154,6 +155,7 @@
     qa[0] = jnp.dot(xn[e], wqkvo[...], preferred_element_type=f32).astype(bf16)
 
     ld_wg.wait()
+    ld_bi.wait()
     ld_sm.wait()
     ld_rt.wait()
     ld_rw.wait()
@@ -169,8 +171,8 @@
     smax_v = smax[...]
     fws, iws = [], []
     for h in range(HN):
-        gi = jnp.sum(gsum[0][h], -1, keepdims=True) + bias_s[0, h]
-        gf = jnp.sum(gsum[1][h], -1, keepdims=True) + bias_s[1, h]
+        gi = jnp.sum(gsum[0][h], -1, keepdims=True) + bias[0:1, h : h + 1]
+        gf = jnp.sum(gsum[1][h], -1, keepdims=True) + bias[1:2, h : h + 1]
         old = jnp.sum(jnp.where(eye, smax_v[h : h + 1, :], 0.0), -1, keepdims=True)
         carried = jnp.minimum(gf, 0.0) - jnp.log(1.0 + jnp.exp(-jnp.abs(gf))) + old
         nm = jnp.maximum(carried, gi)
@@ -459,6 +461,16 @@
     out_max.wait()
 
 
+def store_kernel(*refs):
+    n = len(refs) // 2
+    sem = refs[-1]
+    copies = [pltpu.make_async_copy(refs[i], refs[n + i], sem.at[i]) for i in range(n)]
+    for cp in copies:
+        cp.start()
+    for cp in copies:
+        cp.wait()
+
+
 def per_device(shape, *args):
     (hidden, mgain, wq, wk, wv, wo, wgates, bias, state, snorm, smax, wmix, fgain, routes, rw, eg, eu, ed, sg, su, sd) = args
     E, T = shape["ep"], shape["tp"]
@@ -471,7 +483,7 @@
     f32, bf16 = jnp.float32, jnp.bfloat16
     V, dma = pltpu.VMEM, pltpu.SemaphoreType.DMA
     scratch = [
-        V((S, D), bf16), V((1, D), f32), V((KS, 512), bf16), V((2, HN, D), bf16), V(state.shape, f32), V(snorm.shape, f32),
+        V((S, D), bf16), V((1, D), f32), V((KS, 512), bf16), V((2, HN, D), bf16), V((2, HN), f32), V(state.shape, f32), V(snorm.shape, f32),
         V((HN, S), f32), V(wmix.shape, bf16), V((1, D), f32), V((2, routes.shape[0]), jnp.int32), V((2, S), f32),
         V((2, D // 2, 4 * 128), bf16), V(ed.shape, bf16), V((2 * SW, D), bf16), V((SW, D), bf16),
         V((E, S, KS), bf16), V((E, S, KS), bf16), V((E, S, 512), bf16), V((E, S, 512), bf16),
@@ -487,29 +499,31 @@
         dma((E,)), dma((E,)), dma((Z,)), dma((Z,)), dma((5,)),
     ]
     anywhere = pl.BlockSpec(memory_space=pl.ANY)
-    hbm = pl.BlockSpec(memory_space=pltpu.HBM)
-    in_specs = [hbm] * 21
-    in_specs[7] = pl.BlockSpec(memory_space=pltpu.SMEM)
-    vm = pl.BlockSpec(memory_space=pltpu.VMEM)
-    result, newmat, newnorm, newmax = pl.pallas_call(
+    operands = (
+        hidden, mgain.reshape(1, D), wq, wk, wv, wo, jnp.swapaxes(wgates, 1, 2), bias, state, snorm, smax.T, wmix,
+        fgain.reshape(1, D), routes.T, rw.T, eg, eu, ed, sg.T, su.T, sd,
+    )
+    results = ((S, W), bf16), (state.shape, f32), (snorm.shape, f32), ((HN, S), f32)
+    inner = pl.pallas_call(
         functools.partial(layer_kernel, (EY, EX, Z, S, D, HD, L)),
-        out_shape=(
-            jax.ShapeDtypeStruct((S, W), bf16),
-            jax.ShapeDtypeStruct(state.shape, f32),
-            jax.ShapeDtypeStruct(snorm.shape, f32),
-            jax.ShapeDtypeStruct((HN, S), f32),
-        ),
-        in_specs=in_specs,
-        out_specs=(vm, anywhere, anywhere, anywhere),
+        out_shape=tuple(V(*r) for r in results),
+        in_specs=[anywhere] * len(operands),
+        out_specs=(pl.BlockSpec(memory_space=V), anywhere, anywhere, anywhere),
         scratch_shapes=scratch,
         compiler_params=pltpu.CompilerParams(
             collective_id=0, has_side_effects=True, vmem_limit_bytes=48 * 1024 * 1024
         ),
         name="layer",
-    )(
-        hidden, mgain.reshape(1, D), wq, wk, wv, wo, jnp.swapaxes(wgates, 1, 2), bias, state, snorm, smax.T, wmix,
-        fgain.reshape(1, D), routes.T, rw.T, eg, eu, ed, sg.T, su.T, sd,
-    )
+    )(*(pltpu.with_memory_space_constraint(a, pltpu.HBM) for a in operands))
+    result, newmat, newnorm, newmax = pl.pallas_call(
+        store_kernel,
+        out_shape=tuple(jax.ShapeDtypeStruct(*r) for r in results),
+        in_specs=[anywhere] * len(results),
+        out_specs=(anywhere,) * len(results),
+        scratch_shapes=[dma((len(results),))],
+        compiler_params=pltpu.CompilerParams(vmem_limit_bytes=1024 * 1024),
+        name="store",
+    )(*(pltpu.with_memory_space_constraint(a, V) for a in inner))
     return result, newmat, newnorm, newmax.T
 
 

time: 88.3 us -> 70.4 us (0.80)
  local copies, waits for them, and re-layouts: 17.4 us -> 0 us
    unnamed x38 -> x0, local copies, waits for them, and re-layouts: 17.4 us -> none
    pallas_call x1, Pallas kernels: 69.4 us -> 67.9 us  [per_device(): pl.pallas_call(functools.partial(layer_kernel, (EY, EX, Z, S, D, HD, L)),...]
    pallas_call x0 -> x1, Pallas kernels: none -> 1.37 us  [per_device(): pl.pallas_call(store_kernel, out_shape=tuple((jax.ShapeDtypeStruct(*r) fo...]
where the time goes in v2:
time: 70.4 us; the launch traced here: 69.9 us
  Pallas kernels  69.2 us (98%)
    pallas_call x1, Pallas kernels, per_device(): pl.pallas_call(functools.partial(layer_kernel, (EY, EX, Z, S, D, HD, L)),...  67.9 us

profile of v2, /device:TPU:1, one launch (start us, length us, event | category | flops | bytes accessed | tf_op | source)
XLA Modules:
  0.0 69.9 jit_solution(1889338470501253341)
XLA Ops:
  0.6 67.9 %layer.1 = (bf16[32,256]{1,0:T(8,128)(2,1)S(1)}, f32[32,2,64,64]{3,2,1,0:T(8,128)S(1)}, f32[32,2,64]{2,1,0:T(2,128)S(1)}, f32[2,32]{1,0:T(2,128)S(1)}) custom-call(bf16[32,4096]{1,0:T(8,128)(2,1)} %hidden_h.1, f32[1,4096]{1,0:T(1,128)} %bitcast.12, bf16[256,128]{1,0:T(8,128)(2,1)} %wq_h.1, bf16[256,128]{1,0:T(8,128)(2,1)} %wk_h.1, bf16[256,128]{1,0:T(8,128)(2,1)} %wv_h.1, ...), custom_call_target="tpu_custom_call" | custom-call | tf_op jit(solution)/shard_map/layer/pallas_call | solution.py:507
  68.5 1.4 %store.1 = (bf16[32,256]{1,0:T(8,128)(2,1)}, f32[32,2,64,64]{3,2,1,0:T(8,128)}, f32[32,2,64]{2,1,0:T(2,128)}, f32[2,32]{1,0:T(2,128)}) custom-call(bf16[32,256]{1,0:T(8,128)(2,1)S(1)} %get-tuple-element.12.refs_0_, f32[32,2,64,64]{3,2,1,0:T(8,128)S(1)} %get-tuple-element.13.refs_1_, f32[32,2,64]{2,1,0:T(2,128)S(1)} %get-tuple-element.14.refs_2_, ...), custom_call_target="tpu_custom_call" | custom-call | tf_op jit(solution)/shard_map/store/pallas_call | solution.py:518

commit v3 on v2

v3 whole, which is shorter than its diff:
```python
import functools

import jax
import jax.numpy as jnp
from jax import lax
from jax.experimental import pallas as pl
from jax.experimental.pallas import tpu as pltpu
from jax.sharding import PartitionSpec as P

MESH = pl.DeviceIdType.MESH
NORM_EPS = 1e-06
ROOM = 4


def remote(src, dst, send_sem, recv_sem, dev):
    return pltpu.make_async_remote_copy(
        src_ref=src, dst_ref=dst, send_sem=send_sem, recv_sem=recv_sem, device_id=dev, device_id_type=MESH
    )


def wait_bytes(ref, sem):
    pltpu.make_async_copy(ref, ref, sem).wait()


def far_first(n):
    return sorted(range(1, n), key=lambda i: (-min(i, n - i), i))


def near_first(n):
    return sorted(range(1, n), key=lambda i: (min(i, n - i), i))


def layer_kernel(
    cfg,
    hidden_h, mgain_h, wq_h, wk_h, wv_h, wo_h, wg_h, bias_h, state_h, snorm_h, smax_h, wmix_h, fgain_h,
    routes_h, rw_h, eg_h, eu_h, ed_h, sg_h, su_h, sd_h,
    result_o, newmat_o, newnorm_o, newmax_o,
    hid, mgain, wqkvo, wg, bias, state, snorm, smax, wmix, fgain, routes, rw, wcat, down, sgu, sdown,
    xn, ga, pt, qa, kvq, nums, gated, mixs, mixr, mixm, mixo, rz, so, st, disp, dx, xg, xs, acc, po, pi, ret, rt,
    shs, shr, sho, fin, fz, nnew, mnew,
    lsem, bulk, sends, r1, r2, r3, r4, r5, r6, r7, r8, r9, r10, r11, r12, osem,
):
    EY, EX, Z, S, D, HD, L = cfg
    E, T = EY * EX, 2 * Z
    W = D // T
    f32, bf16 = jnp.float32, jnp.bfloat16
    e, t = lax.axis_index("ep"), lax.axis_index("tp")
    z, c = lax.div(t, 2), lax.rem(t, 2)
    o = 1 - c
    sib = (e, z * 2 + o)
    y, x = lax.div(e, EX), lax.rem(e, EX)
    s1, s2, s3, s4, s5, s6, s7, s8, s9, s10, s11, s12 = (sends.at[k] for k in range(12))

    def ep_peer(i):
        return lax.rem(y + lax.div(i, EX), EY) * EX + lax.rem(x + lax.rem(i, EX), EX)

    def ep_src(i):
        return lax.rem(y + EY - lax.div(i, EX), EY) * EX + lax.rem(x + EX - lax.rem(i, EX), EX)

    def z_dev(zz):
        return (e, zz * 2 + c)

    def zp(i):
        return lax.rem(z + i, Z)

    def zs(i):
        return lax.rem(z + Z - i, Z)

    def col(zz, cc):
        return pl.ds(pl.multiple_of((zz * 2 + cc) * W, W), W)

    def half(zz):
        return pl.ds(pl.multiple_of(zz * W, W), W)

    def rows(g):
        return pl.ds(pl.multiple_of(g * L * ROOM, L * ROOM), L * ROOM)

    def each(first, n, step):
        def one(i, _):
            step(i)
            return 0

        lax.fori_loop(first, n, one, 0)

    barrier = pltpu.get_barrier_semaphore()

    def greet(dev):
        pl.semaphore_signal(barrier, inc=1, device_id=dev, device_id_type=MESH)

    loads = []

    def load(src, dst):
        cp = pltpu.make_async_copy(src, dst, lsem.at[len(loads)])
        cp.start()
        loads.append(cp)
        return cp

    ld_hid = load(hidden_h, hid)
    ld_mg = load(mgain_h, mgain)
    each(1, E, lambda i: greet((ep_peer(i), t)))
    for i in far_first(Z):
        greet(z_dev(zp(i)))
    greet(sib)
    for k, w in enumerate((wq_h, wk_h, wv_h, wo_h)):
        pltpu.make_async_copy(w, wqkvo.at[:, k * 128 : (k + 1) * 128], bulk.at[0]).start()

    ld_hid.wait()
    ld_mg.wait()
    KS = D // E
    sq = jnp.zeros((S, 128), f32)
    for k in range(D // 128):
        v = hid[:, k * 128 : (k + 1) * 128].astype(f32)
        sq = sq + v * v
    scale = lax.rsqrt(jnp.sum(sq, -1, keepdims=True) * (1.0 / D) + NORM_EPS)
    for k in range(E):
        v = hid[:, k * KS : (k + 1) * KS].astype(f32)
        xn[k] = (v * scale * mgain[:, k * KS : (k + 1) * KS]).astype(bf16)
    pl.semaphore_wait(barrier, E - 1 + Z - 1 + 1)

    def send_x(i):
        p = ep_peer(i)
        remote(xn.at[p], ga.at[e], s1, r1.at[i], (p, t)).start()

    each(1, E, send_x)

    ld_wg = load(wg_h, wg)
    ld_bi = load(bias_h, bias)
    ld_sm = load(smax_h, smax)
    ld_rt = load(routes_h, routes)
    ld_rw = load(rw_h, rw)
    ld_sn = load(snorm_h, snorm)
    ld_st = load(state_h, state)
    ld_fg = load(fgain_h, fgain)
    SW = sg_h.shape[0]

    def start_narrow(k):
        zz, cc = lax.div(k, 2), lax.rem(k, 2)
        cols = pl.ds(pl.multiple_of(k * W, W), W)
        pltpu.make_async_copy(wmix_h.at[:, cols], wmix.at[cc, :, half(zz)], bulk.at[1]).start()
        pltpu.make_async_copy(sg_h.at[:, cols], sgu.at[cc, 0:SW, half(zz)], bulk.at[2]).start()
        pltpu.make_async_copy(su_h.at[:, cols], sgu.at[cc, SW : 2 * SW, half(zz)], bulk.at[2]).start()
        pltpu.make_async_copy(sd_h.at[:, cols], sdown.at[cc, :, half(zz)], bulk.at[3]).start()

    def start_wide(k):
        zz, cc = lax.div(k, 2), lax.rem(k, 2)
        cols = pl.ds(pl.multiple_of(k * W, W), W)
        for j in range(L):
            for q, src in enumerate((eg_h, eu_h)):
                lanes = slice((2 * j + q) * 128, (2 * j + q + 1) * 128)
                pltpu.make_async_copy(src.at[j, cols, :], wcat.at[cc, half(zz), lanes], bulk.at[4]).start()
            pltpu.make_async_copy(
                ed_h.at[j, :, cols], down.at[cc, j * 128 : (j + 1) * 128, half(zz)], bulk.at[5]
            ).start()

    each(0, T, start_narrow)
    each(0, T, start_wide)

    wait_bytes(wqkvo, bulk.at[0])
    qa[0] = jnp.dot(xn[e], wqkvo[...], preferred_element_type=f32).astype(bf16)

    def project(i):
        g = ep_src(i)
        remote(xn.at[g], ga.at[g], s1, r1.at[i], (g, t)).wait_recv()
        pt[g] = jnp.dot(ga[g], wqkvo[...], preferred_element_type=f32).astype(bf16)
        remote(pt.at[g], qa.at[i], s2, r2.at[0], (g, t)).start()

    each(1, E, project)

    ld_wg.wait()
    ld_bi.wait()
    ld_sm.wait()
    ld_rt.wait()
    ld_rw.wait()
    HN = 2
    gsum = [[jnp.zeros((S, 128), f32) for _ in range(HN)] for _ in range(2)]
    for k in range(D // 128):
        v = xn[k * 128 // KS, :, (k * 128) % KS : (k * 128) % KS + 128].astype(f32)
        for g in range(2):
            w2 = wg[g, :, k * 128 : (k + 1) * 128].astype(f32)
            for h in range(HN):
                gsum[g][h] = gsum[g][h] + v * w2[h : h + 1, :]
    eye = lax.broadcasted_iota(jnp.int32, (S, S), 0) == lax.broadcasted_iota(jnp.int32, (S, S), 1)
    smax_v = smax[...]
    fws, iws = [], []
    for h in range(HN):
        gi = jnp.sum(gsum[0][h], -1, keepdims=True) + bias[0:1, h : h + 1]
        gf = jnp.sum(gsum[1][h], -1, keepdims=True) + bias[1:2, h : h + 1]
        old = jnp.sum(jnp.where(eye, smax_v[h : h + 1, :], 0.0), -1, keepdims=True)
        carried = jnp.minimum(gf, 0.0) - jnp.log(1.0 + jnp.exp(-jnp.abs(gf))) + old
        nm = jnp.maximum(carried, gi)
        fws.append(jnp.exp(carried - nm))
        iws.append(jnp.exp(gi - nm))
        mnew[h : h + 1, :] = jnp.sum(jnp.where(eye, nm, 0.0), 0, keepdims=True)
    out_max = pltpu.make_async_copy(mnew, newmax_o, osem.at[2])
    out_max.start()

    GR = routes_h.shape[1]
    sel = (
        lax.broadcasted_iota(jnp.int32, (S, GR), 1) == lax.broadcasted_iota(jnp.int32, (S, GR), 0) + e * S
    )
    all_routes = routes[...].astype(f32)
    sel_f = jnp.where(sel, 1.0, 0.0)
    r_col = [jnp.sum(sel_f * all_routes[j : j + 1, :], -1, keepdims=True) for j in range(2)]
    r_row = [jnp.sum(jnp.where(eye, r_col[j], 0.0), 0, keepdims=True) for j in range(2)]
    i0 = lax.broadcasted_iota(jnp.int32, (S, S), 0)
    i1 = lax.broadcasted_iota(jnp.int32, (S, S), 1)
    NS = E * L * ROOM
    slot_row, slot_col = [], []
    for j in range(2):
        same = jnp.where(r_col[0] == r_row[j], 1.0, 0.0) + jnp.where(r_col[1] == r_row[j], 1.0, 0.0)
        rank_row = jnp.sum(jnp.where(i0 < i1, same, 0.0), 0, keepdims=True)
        slot_row.append(r_row[j] * ROOM + rank_row)
        same = jnp.where(r_row[0] == r_col[j], 1.0, 0.0) + jnp.where(r_row[1] == r_col[j], 1.0, 0.0)
        rank_col = jnp.sum(jnp.where(i1 < i0, same, 0.0), -1, keepdims=True)
        slot_col.append(r_col[j] * ROOM + rank_col)
    slot_ids = lax.broadcasted_iota(jnp.int32, (NS, S), 0).astype(f32)
    chooser = jnp.where((slot_ids == slot_row[0]) | (slot_ids == slot_row[1]), 1.0, 0.0).astype(bf16)
    rw_v = rw[...]
    rw_col = [jnp.sum(jnp.where(eye, rw_v[j : j + 1, :], 0.0), -1, keepdims=True) for j in range(2)]
    lane_ids = lax.broadcasted_iota(jnp.int32, (S, NS), 1).astype(f32)
    wsel = jnp.where(lane_ids == slot_col[0], rw_col[0], 0.0) + jnp.where(lane_ids == slot_col[1], rw_col[1], 0.0)
    w_hi = wsel.astype(bf16)
    w_lo = (wsel - w_hi.astype(f32)).astype(bf16)
    w_both = jnp.concatenate([w_hi, w_lo], 0)

    ld_sn.wait()
    ld_st.wait()
    wait_bytes(qa.at[pl.ds(1, E - 1)], r2.at[0])
    roles = []
    for k in range(4):
        total = qa[0, :, k * 128 : (k + 1) * 128].astype(f32)
        for i in range(1, E):
            total = total + qa[i, :, k * 128 : (k + 1) * 128].astype(f32)
        roles.append(total.astype(bf16).astype(f32))

    for h in range(HN):
        hs = slice(h * HD, (h + 1) * HD)
        qh, kh, vh = roles[0][:, hs], roles[1][:, hs] * HD ** (-0.5), roles[2][:, hs]
        kvq[h, 0] = qh
        kvq[h, 1] = kh
        kvq[h, 2] = vh * iws[h]
        kvq[h, 3] = jnp.broadcast_to(fws[h], (S, HD))
    SB = 8

    def cell(b):
        at = pl.ds(pl.multiple_of(b * SB, SB), SB)
        for h in range(HN):
            new = (
                kvq[h, 3, at, :][:, None, :] * state[at, h]
                + kvq[h, 2, at, :][:, :, None] * kvq[h, 1, at, :][:, None, :]
            )
            state[at, h] = new
            nums[h, at, :] = jnp.sum(new * kvq[h, 0, at, :][:, None, :], -1)

    each(0, S // SB, cell)
    out_mat = pltpu.make_async_copy(state, newmat_o, osem.at[0])
    out_mat.start()
    for h in range(HN):
        hs = slice(h * HD, (h + 1) * HD)
        nn = fws[h] * snorm[:, h, :] + iws[h] * kvq[h, 1]
        nnew[:, h, :] = nn
        den = jnp.maximum(jnp.abs(jnp.sum(nn * kvq[h, 0], -1, keepdims=True)), 1.0)
        gate = 1.0 / (1.0 + jnp.exp(-roles[3][:, hs]))
        gated[:, hs] = (gate * nums[h] / den).astype(bf16)
    out_norm = pltpu.make_async_copy(nnew, newnorm_o, osem.at[1])
    out_norm.start()

    wait_bytes(wmix, bulk.at[1])
    gv = gated[...]
    zorder = far_first(Z) + [0]
    theirs = jnp.dot(gv, wmix[o], preferred_element_type=f32)
    for zz in range(Z):
        mixs[zz] = theirs[:, zz * W : (zz + 1) * W].astype(bf16)
    for i in zorder:
        remote(mixs.at[zp(i)], mixr.at[zp(i)], s3, r3.at[i], sib).start()
    mine = jnp.dot(gv, wmix[c], preferred_element_type=f32)
    for zz in range(Z):
        mixm[zz] = mine[:, zz * W : (zz + 1) * W]
    own = None
    for i in zorder:
        zz = zp(i)
        remote(mixs.at[zz], mixr.at[zz], s3, r3.at[i], sib).wait_recv()
        both = mixm[zz] + mixr[zz].astype(f32)
        if i:
            mixo[i] = both.astype(bf16)
            remote(mixo.at[i], rz.at[i], s4, r4.at[0], z_dev(zz)).start()
        else:
            own = both
    own = own + hid[:, pl.ds(pl.multiple_of(t * W, W), W)].astype(f32)
    wait_bytes(rz.at[pl.ds(1, Z - 1)], r4.at[0])
    for i in range(1, Z):
        own = own + rz[i].astype(f32)
    so[...] = own.astype(bf16)

    for i in far_first(Z):
        remote(so, st.at[c, z], s5, r5.at[i], z_dev(zp(i))).start()

    def dispatch(block, g):
        disp[:, half(g)] = jnp.dot(chooser, block, preferred_element_type=f32).astype(bf16)

        def send_rows(i):
            p = ep_peer(i)
            remote(disp.at[rows(p), half(g)], dx.at[c, rows(e), half(g)], s7, r7.at[i], (p, t)).start()

        each(1, E, send_rows)
        pltpu.make_async_copy(disp.at[rows(e), half(g)], dx.at[c, rows(e), half(g)], r7.at[0]).start()

    dispatch(so[...], z)
    remote(so, st.at[c, z], s6, r6.at[0], sib).start()
    st[c, z] = so[...]
    for i in near_first(Z):
        g = zs(i)
        remote(so, st.at[c, g], s5, r5.at[i], z_dev(g)).wait_recv()
        dispatch(st[c, g], g)
        remote(st.at[c, g], st.at[c, g], s6, r6.at[0], sib).start()

    ld_fg.wait()
    wait_bytes(sgu, bulk.at[2])
    wait_bytes(sdown, bulk.at[3])
    wait_bytes(st.at[o], r6.at[0])
    sq = jnp.zeros((S, W), f32)
    for cc in range(2):
        for zz in range(Z):
            v = st[cc, zz].astype(f32)
            sq = sq + v * v
    sscale = lax.rsqrt(jnp.sum(sq, -1, keepdims=True) * (1.0 / D) + NORM_EPS)
    pre = jnp.zeros((S, 2 * SW), f32)
    for cc in range(2):
        for zz in range(Z):
            cs = slice((zz * 2 + cc) * W, (zz * 2 + cc + 1) * W)
            xs[:, zz * W : (zz + 1) * W] = (st[cc, zz].astype(f32) * sscale * fgain[:, cs]).astype(bf16)
        pre = pre + lax.dot_general(xs[...], sgu[cc], (((1,), (1,)), ((), ())), preferred_element_type=f32)
    sgate, sup = pre[:, :SW], pre[:, SW:]
    shid = (sgate / (1.0 + jnp.exp(-sgate)) * sup).astype(bf16)
    theirs = jnp.dot(shid, sdown[o], preferred_element_type=f32)
    for zz in range(Z):
        shs[zz] = theirs[:, zz * W : (zz + 1) * W].astype(bf16)
    remote(shs, shr, s9, r9.at[0], sib).start()
    mine = jnp.dot(shid, sdown[c], preferred_element_type=f32)
    for zz in range(Z):
        sho[zz] = mine[:, zz * W : (zz + 1) * W]

    def pass_on(i):
        g = ep_src(i)
        wait_bytes(dx.at[c, rows(g)], r7.at[i])
        remote(dx.at[c, rows(g)], dx.at[c, rows(g)], s8, r8.at[0], sib).start()

    each(0, E, pass_on)
    wait_bytes(wcat, bulk.at[4])

    def prepare(cc, sq):
        def piece(zz, sq):
            v = dx[cc, :, half(zz)].astype(f32)
            xg[:, half(zz)] = (v * fgain[:, col(zz, cc)]).astype(bf16)
            v = v * v
            for k in range(W // 128):
                sq = sq + v[:, k * 128 : (k + 1) * 128]
            return sq

        return lax.fori_loop(0, Z, piece, sq)

    sq = prepare(c, jnp.zeros((NS, 128), f32))
    acc[...] = jnp.dot(xg[...], wcat[c], preferred_element_type=f32)
    wait_bytes(dx.at[o], r8.at[0])
    sq = prepare(o, sq)
    acc[...] += jnp.dot(xg[...], wcat[o], preferred_element_type=f32)
    escale = lax.rsqrt(jnp.sum(sq, -1, keepdims=True) * (1.0 / D) + NORM_EPS)
    expert_of = lax.rem(lax.div(lax.broadcasted_iota(jnp.int32, (NS, 128), 0), ROOM), L)
    hids = []
    for j in range(L):
        gv = acc[:, 2 * j * 128 : (2 * j + 1) * 128] * escale
        uv = acc[:, (2 * j + 1) * 128 : (2 * j + 2) * 128] * escale
        hids.append(jnp.where(expert_of == j, gv / (1.0 + jnp.exp(-gv)) * uv, 0.0).astype(bf16))
    hcat = jnp.concatenate(hids, 1)

    wait_bytes(down, bulk.at[5])
    LAG = min(3, Z)

    def down_theirs(i):
        zz = zp(i)
        po[i] = jnp.dot(hcat, down[o, :, half(zz)], preferred_element_type=f32).astype(bf16)
        remote(po.at[i], pi.at[i], s10, r10.at[i], sib).start()

    def down_mine(i):
        zz = zp(i)
        part = jnp.dot(hcat, down[c, :, half(zz)], preferred_element_type=f32)
        remote(po.at[i], pi.at[i], s10, r10.at[i], sib).wait_recv()
        ret[:, half(zz)] = (part + pi[i].astype(f32)).astype(bf16)

        def send_back(k):
            p = ep_peer(k)
            remote(ret.at[rows(p), half(zz)], rt.at[rows(e), half(zz)], s11, r11.at[i], (p, t)).start()

        each(1, E, send_back)
        pltpu.make_async_copy(ret.at[rows(e), half(zz)], rt.at[rows(e), half(zz)], r11.at[i]).start()

    for k in range(Z + LAG):
        if k < Z:
            down_theirs(zorder[k])
        if k >= LAG:
            down_mine(zorder[k - LAG])

    remote(shs, shr, s9, r9.at[0], sib).wait_recv()
    own = None
    for i in zorder:
        zz = zp(i)
        wait_bytes(rt.at[:, half(zz)], r11.at[i])
        two = jnp.dot(w_both, rt[:, half(zz)], preferred_element_type=f32)
        both = two[:S] + two[S:] + sho[zz] + shr[zz].astype(f32)
        if i:
            fin[i] = both.astype(bf16)
            remote(fin.at[i], fz.at[i], s12, r12.at[0], z_dev(zz)).start()
        else:
            own = both
    own = own + so[...].astype(f32)
    wait_bytes(fz.at[pl.ds(1, Z - 1)], r12.at[0])
    for i in range(1, Z):
        own = own + fz[i].astype(f32)
    result_o[...] = own.astype(bf16)

    wait_bytes(xn.at[pl.ds(1, E - 1)], s1)
    wait_bytes(pt.at[pl.ds(1, E - 1)], s2)
    wait_bytes(mixs, s3)
    wait_bytes(mixo.at[pl.ds(1, Z - 1)], s4)
    wait_bytes(mixo.at[pl.ds(1, Z - 1)], s5)
    wait_bytes(mixs, s6)
    wait_bytes(disp.at[pl.ds(0, NS - L * ROOM)], s7)
    wait_bytes(disp, s8)
    wait_bytes(shs, s9)
    wait_bytes(po, s10)
    wait_bytes(ret.at[pl.ds(0, NS - L * ROOM)], s11)
    wait_bytes(fin.at[pl.ds(1, Z - 1)], s12)
    out_mat.wait()
    out_norm.wait()
    out_max.wait()


def store_kernel(*refs):
    n = len(refs) // 2
    sem = refs[-1]
    copies = [pltpu.make_async_copy(refs[i], refs[n + i], sem.at[i]) for i in range(n)]
    for cp in copies:
        cp.start()
    for cp in copies:
        cp.wait()


def per_device(shape, *args):
    (hidden, mgain, wq, wk, wv, wo, wgates, bias, state, snorm, smax, wmix, fgain, routes, rw, eg, eu, ed, sg, su, sd) = args
    E, T = shape["ep"], shape["tp"]
    EX = 4 if E % 4 == 0 and E > 4 else 2
    EY, Z = E // EX, T // 2
    S, D = hidden.shape
    HN, HD = state.shape[1], state.shape[2]
    L, SW = eg.shape[0], sg.shape[1]
    W, KS, NS = D // T, D // E, E * L * ROOM
    f32, bf16 = jnp.float32, jnp.bfloat16
    V, dma = pltpu.VMEM, pltpu.SemaphoreType.DMA
    H = D // 2
    scratch = [
        V((S, D), bf16), V((1, D), f32), V((KS, 512), bf16), V((2, HN, D), bf16), V((2, HN), f32), V(state.shape, f32),
        V(snorm.shape, f32), V((HN, S), f32), V((2, wmix.shape[0], H), bf16), V((1, D), f32),
        V((2, routes.shape[0]), jnp.int32), V((2, S), f32), V((2, H, 4 * 128), bf16), V((2, L * 128, H), bf16),
        V((2, 2 * SW, H), bf16), V((2, SW, H), bf16),
        V((E, S, KS), bf16), V((E, S, KS), bf16), V((E, S, 512), bf16), V((E, S, 512), bf16),
        V((HN, 4, S, HD), f32), V((HN, S, HD), f32), V((S, HN * HD), bf16),
        V((Z, S, W), bf16), V((Z, S, W), bf16), V((Z, S, W), f32), V((Z, S, W), bf16), V((Z, S, W), bf16),
        V((S, W), bf16), V((2, Z, S, W), bf16), V((NS, H), bf16), V((2, NS, H), bf16), V((NS, H), bf16), V((S, H), bf16),
        V((NS, 512), f32), V((Z, NS, W), bf16), V((Z, NS, W), bf16), V((NS, H), bf16), V((NS, H), bf16),
        V((Z, S, W), bf16), V((Z, S, W), bf16), V((Z, S, W), f32), V((Z, S, W), bf16), V((Z, S, W), bf16),
        V(snorm.shape, f32), V((HN, S), f32),
        dma((10,)), dma((6,)), dma((12,)),
        dma((E,)), dma((1,)), dma((Z,)), dma((1,)), dma((Z,)), dma((1,)), dma((E,)), dma((1,)), dma((1,)), dma((Z,)),
        dma((Z,)), dma((1,)), dma((3,)),
    ]
    anywhere = pl.BlockSpec(memory_space=pl.ANY)
    operands = (
        hidden, mgain.reshape(1, D), wq, wk, wv, wo, jnp.swapaxes(wgates, 1, 2), bias, state, snorm, smax.T, wmix,
        fgain.reshape(1, D), routes.T, rw.T, eg, eu, ed, sg.T, su.T, sd,
    )
    results = ((S, W), bf16), (state.shape, f32), (snorm.shape, f32), ((HN, S), f32)
    inner = pl.pallas_call(
        functools.partial(layer_kernel, (EY, EX, Z, S, D, HD, L)),
        out_shape=tuple(V(*r) for r in results),
        in_specs=[anywhere] * len(operands),
        out_specs=(pl.BlockSpec(memory_space=V), anywhere, anywhere, anywhere),
        scratch_shapes=scratch,
        compiler_params=pltpu.CompilerParams(
            collective_id=0, has_side_effects=True, vmem_limit_bytes=48 * 1024 * 1024
        ),
        name="layer",
    )(*(pltpu.with_memory_space_constraint(a, pltpu.HBM) for a in operands))
    result, newmat, newnorm, newmax = pl.pallas_call(
        store_kernel,
        out_shape=tuple(jax.ShapeDtypeStruct(*r) for r in results),
        in_specs=[anywhere] * len(results),
        out_specs=(anywhere,) * len(results),
        scratch_shapes=[dma((len(results),))],
        compiler_params=pltpu.CompilerParams(vmem_limit_bytes=1024 * 1024),
        name="store",
    )(*(pltpu.with_memory_space_constraint(a, V) for a in inner))
    return result, newmat, newnorm, newmax.T


def solution(mesh):
    placed = (
        P("ep", None),
        P(),
        P("ep", "tp"),
        P("ep", "tp"),
        P("ep", "tp"),
        P("ep", "tp"),
        P(None, None, "tp"),
        P(None, "tp"),
        P("ep", "tp", None, None),
        P("ep", "tp", None),
        P("ep", "tp"),
        P("tp", None),
        P(),
        P(),
        P("ep", None),
        P("ep", None, "tp"),
        P("ep", None, "tp"),
        P("ep", "tp", None),
        P(None, "tp"),
        P(None, "tp"),
        P("tp", None),
    )
    return jax.shard_map(
        functools.partial(per_device, dict(mesh.shape)),
        mesh=mesh,
        in_specs=placed,
        out_specs=(P("ep", "tp"), P("ep", "tp", None, None), P("ep", "tp", None), P("ep", "tp")),
        check_vma=False,
    )
```

time: 70.4 us -> 62.8 us (0.89)
  Pallas kernels: 69.2 us -> 62.1 us
    pallas_call x1, Pallas kernels: 67.9 us -> 60.7 us  [per_device(): pl.pallas_call(functools.partial(layer_kernel, (EY, EX, Z, S, D, HD, L)),...]
where the time goes in v3:
time: 62.8 us; the launch traced here: 62.7 us
  Pallas kernels  62.1 us (99%)
  between operations  0.65 us (1%)
    pallas_call x1, Pallas kernels, per_device(): pl.pallas_call(functools.partial(layer_kernel, (EY, EX, Z, S, D, HD, L)),...  60.7 us
    pallas_call x1, Pallas kernels, per_device(): pl.pallas_call(store_kernel, out_shape=tuple((jax.ShapeDtypeStruct(*r) fo...  1.37 us

profile of v3, /device:TPU:1, one launch (start us, length us, event | category | flops | bytes accessed | tf_op | source)
XLA Modules:
  0.0 62.7 jit_solution(8050971241148023346)
XLA Ops:
  0.6 60.7 %layer.1 = (bf16[32,256]{1,0:T(8,128)(2,1)S(1)}, f32[32,2,64,64]{3,2,1,0:T(8,128)S(1)}, f32[32,2,64]{2,1,0:T(2,128)S(1)}, f32[2,32]{1,0:T(2,128)S(1)}) custom-call(bf16[32,4096]{1,0:T(8,128)(2,1)} %hidden_h.1, f32[1,4096]{1,0:T(1,128)} %bitcast.12, bf16[256,128]{1,0:T(8,128)(2,1)} %wq_h.1, bf16[256,128]{1,0:T(8,128)(2,1)} %wk_h.1, bf16[256,128]{1,0:T(8,128)(2,1)} %wv_h.1, ...), custom_call_target="tpu_custom_call" | custom-call | tf_op jit(solution)/shard_map/layer/pallas_call | solution.py:482
  61.3 1.4 %store.1 = (bf16[32,256]{1,0:T(8,128)(2,1)}, f32[32,2,64,64]{3,2,1,0:T(8,128)}, f32[32,2,64]{2,1,0:T(2,128)}, f32[2,32]{1,0:T(2,128)}) custom-call(bf16[32,256]{1,0:T(8,128)(2,1)S(1)} %get-tuple-element.12.refs_0_, f32[32,2,64,64]{3,2,1,0:T(8,128)S(1)} %get-tuple-element.13.refs_1_, f32[32,2,64]{2,1,0:T(2,128)S(1)} %get-tuple-element.14.refs_2_, ...), custom_call_target="tpu_custom_call" | custom-call | tf_op jit(solution)/shard_map/store/pallas_call | solution.py:493

commit v4 on v3

--- a/solution.py
+++ b/solution.py
@@ -9,6 +9,8 @@
 
 MESH = pl.DeviceIdType.MESH
 NORM_EPS = 1e-06
+ORDER_A = (1, 4, 3, 2)
+ORDER_B = (1, 2, 4, 3)
 ROOM = 4
 
 
@@ -24,6 +26,14 @@
 
 def far_first(n):
     return sorted(range(1, n), key=lambda i: (-min(i, n - i), i))
+
+
+def by_hops(ey, ex, order):
+    def hops(i):
+        dy, dx = i // ex, i % ex
+        return min(dy, ey - dy) + min(dx, ex - dx)
+
+    return [i for h in order for i in range(1, ey * ex) if hops(i) == h]
 
 
 def near_first(n):
@@ -36,7 +46,7 @@
     routes_h, rw_h, eg_h, eu_h, ed_h, sg_h, su_h, sd_h,
     result_o, newmat_o, newnorm_o, newmax_o,
     hid, mgain, wqkvo, wg, bias, state, snorm, smax, wmix, fgain, routes, rw, wcat, down, sgu, sdown,
-    xn, ga, pt, qa, kvq, nums, gated, mixs, mixr, mixm, mixo, rz, so, st, disp, dx, xg, xs, acc, po, pi, ret, rt,
+    xn, ga, pt, qa, kvq, nums, gated, mixs, mixr, mixm, mixo, rz, so, st, disp, dx, xs, acc, sqs, po, pi, ret, rt,
     shs, shr, sho, fin, fz, nnew, mnew,
     lsem, bulk, sends, r1, r2, r3, r4, r5, r6, r7, r8, r9, r10, r11, r12, osem,
 ):
@@ -57,6 +67,13 @@
     def ep_src(i):
         return lax.rem(y + EY - lax.div(i, EX), EY) * EX + lax.rem(x + EX - lax.rem(i, EX), EX)
 
+    ypart = [lax.rem(y + k, EY) * EX for k in range(EY)]
+    xpart = [lax.rem(x + k, EX) for k in range(EX)]
+    peers = [None] + [ypart[i // EX] + xpart[i % EX] for i in range(1, E)]
+    ep_far = by_hops(EY, EX, (4, 3, 2, 1))
+    ep_sent = by_hops(EY, EX, ORDER_A)
+    ep_done = by_hops(EY, EX, ORDER_B)
+
     def z_dev(zz):
         return (e, zz * 2 + c)
 
@@ -118,10 +135,11 @@
     pl.semaphore_wait(barrier, E - 1 + Z - 1 + 1)
 
     def send_x(i):
-        p = ep_peer(i)
+        p = peers[i]
         remote(xn.at[p], ga.at[e], s1, r1.at[i], (p, t)).start()
 
-    each(1, E, send_x)
+    for i in ep_sent:
+        send_x(i)
 
     ld_wg = load(wg_h, wg)
     ld_bi = load(bias_h, bias)
@@ -164,7 +182,8 @@
         pt[g] = jnp.dot(ga[g], wqkvo[...], preferred_element_type=f32).astype(bf16)
         remote(pt.at[g], qa.at[i], s2, r2.at[0], (g, t)).start()
 
-    each(1, E, project)
+    for i in ep_done:
+        project(i)
 
     ld_wg.wait()
     ld_bi.wait()
@@ -253,8 +272,6 @@
             nums[h, at, :] = jnp.sum(new * kvq[h, 0, at, :][:, None, :], -1)
 
     each(0, S // SB, cell)
-    out_mat = pltpu.make_async_copy(state, newmat_o, osem.at[0])
-    out_mat.start()
     for h in range(HN):
         hs = slice(h * HD, (h + 1) * HD)
         nn = fws[h] * snorm[:, h, :] + iws[h] * kvq[h, 1]
@@ -262,8 +279,6 @@
         den = jnp.maximum(jnp.abs(jnp.sum(nn * kvq[h, 0], -1, keepdims=True)), 1.0)
         gate = 1.0 / (1.0 + jnp.exp(-roles[3][:, hs]))
         gated[:, hs] = (gate * nums[h] / den).astype(bf16)
-    out_norm = pltpu.make_async_copy(nnew, newnorm_o, osem.at[1])
-    out_norm.start()
 
     wait_bytes(wmix, bulk.at[1])
     gv = gated[...]
@@ -286,6 +301,10 @@
             remote(mixo.at[i], rz.at[i], s4, r4.at[0], z_dev(zz)).start()
         else:
             own = both
+    out_mat = pltpu.make_async_copy(state, newmat_o, osem.at[0])
+    out_mat.start()
+    out_norm = pltpu.make_async_copy(nnew, newnorm_o, osem.at[1])
+    out_norm.start()
     own = own + hid[:, pl.ds(pl.multiple_of(t * W, W), W)].astype(f32)
     wait_bytes(rz.at[pl.ds(1, Z - 1)], r4.at[0])
     for i in range(1, Z):
@@ -295,23 +314,20 @@
     for i in far_first(Z):
         remote(so, st.at[c, z], s5, r5.at[i], z_dev(zp(i))).start()
 
-    def dispatch(block, g):
-        disp[:, half(g)] = jnp.dot(chooser, block, preferred_element_type=f32).astype(bf16)
-
-        def send_rows(i):
-            p = ep_peer(i)
-            remote(disp.at[rows(p), half(g)], dx.at[c, rows(e), half(g)], s7, r7.at[i], (p, t)).start()
-
-        each(1, E, send_rows)
-        pltpu.make_async_copy(disp.at[rows(e), half(g)], dx.at[c, rows(e), half(g)], r7.at[0]).start()
-
-    dispatch(so[...], z)
+    def dispatch(block, i):
+        g = zs(i)
+        disp[g] = jnp.dot(chooser, block, preferred_element_type=f32).astype(bf16)
+        for k in ep_far:
+            remote(disp.at[g, rows(peers[k])], dx.at[c, g, rows(e)], s7, r7.at[i], (peers[k], t)).start()
+        pltpu.make_async_copy(disp.at[g, rows(e)], dx.at[c, g, rows(e)], r7.at[i]).start()
+
+    dispatch(so[...], 0)
     remote(so, st.at[c, z], s6, r6.at[0], sib).start()
     st[c, z] = so[...]
     for i in near_first(Z):
         g = zs(i)
         remote(so, st.at[c, g], s5, r5.at[i], z_dev(g)).wait_recv()
-        dispatch(st[c, g], g)
+        dispatch(st[c, g], i)
         remote(st.at[c, g], st.at[c, g], s6, r6.at[0], sib).start()
 
     ld_fg.wait()
@@ -340,30 +356,32 @@
     for zz in range(Z):
         sho[zz] = mine[:, zz * W : (zz + 1) * W]
 
-    def pass_on(i):
-        g = ep_src(i)
-        wait_bytes(dx.at[c, rows(g)], r7.at[i])
-        remote(dx.at[c, rows(g)], dx.at[c, rows(g)], s8, r8.at[0], sib).start()
-
-    each(0, E, pass_on)
     wait_bytes(wcat, bulk.at[4])
-
-    def prepare(cc, sq):
-        def piece(zz, sq):
-            v = dx[cc, :, half(zz)].astype(f32)
-            xg[:, half(zz)] = (v * fgain[:, col(zz, cc)]).astype(bf16)
-            v = v * v
-            for k in range(W // 128):
-                sq = sq + v[:, k * 128 : (k + 1) * 128]
-            return sq
-
-        return lax.fori_loop(0, Z, piece, sq)
-
-    sq = prepare(c, jnp.zeros((NS, 128), f32))
-    acc[...] = jnp.dot(xg[...], wcat[c], preferred_element_type=f32)
-    wait_bytes(dx.at[o], r8.at[0])
-    sq = prepare(o, sq)
-    acc[...] += jnp.dot(xg[...], wcat[o], preferred_element_type=f32)
+    acc[...] = jnp.zeros_like(acc)
+    sqs[...] = jnp.zeros_like(sqs)
+
+    def block_of(cc, g):
+        v = dx[cc, g].astype(f32)
+        scaled = (v * fgain[:, col(g, cc)]).astype(bf16)
+        acc[...] += jnp.dot(scaled, wcat[cc, half(g), :], preferred_element_type=f32)
+        v = v * v
+        sqs[...] += sum(v[:, k * 128 : (k + 1) * 128] for k in range(W // 128))
+
+    arrivals = [0] + near_first(Z)
+    BEHIND = min(2, Z)
+    for k in range(Z + BEHIND):
+        if k < Z:
+            i = arrivals[k]
+            g = zs(i)
+            wait_bytes(dx.at[c, g], r7.at[i])
+            remote(dx.at[c, g], dx.at[c, g], s8, r8.at[i], sib).start()
+            block_of(c, g)
+        if k >= BEHIND:
+            i = arrivals[k - BEHIND]
+            g = zs(i)
+            remote(dx.at[c, g], dx.at[o, g], s8, r8.at[i], sib).wait_recv()
+            block_of(o, g)
+    sq = sqs[...]
     escale = lax.rsqrt(jnp.sum(sq, -1, keepdims=True) * (1.0 / D) + NORM_EPS)
     expert_of = lax.rem(lax.div(lax.broadcasted_iota(jnp.int32, (NS, 128), 0), ROOM), L)
     hids = []
@@ -385,14 +403,13 @@
         zz = zp(i)
         part = jnp.dot(hcat, down[c, :, half(zz)], preferred_element_type=f32)
         remote(po.at[i], pi.at[i], s10, r10.at[i], sib).wait_recv()
-        ret[:, half(zz)] = (part + pi[i].astype(f32)).astype(bf16)
-
-        def send_back(k):
-            p = ep_peer(k)
-            remote(ret.at[rows(p), half(zz)], rt.at[rows(e), half(zz)], s11, r11.at[i], (p, t)).start()
-
-        each(1, E, send_back)
-        pltpu.make_async_copy(ret.at[rows(e), half(zz)], rt.at[rows(e), half(zz)], r11.at[i]).start()
+        ret[i] = (part + pi[i].astype(f32)).astype(bf16)
+
+        for k in ep_far:
+            p = peers[k]
+            remote(ret.at[i, rows(p)], rt.at[i, rows(e)], s11, r11.at[i], (p, t)).start()
+
+        pltpu.make_async_copy(ret.at[i, rows(e)], rt.at[i, rows(e)], r11.at[i]).start()
 
     for k in range(Z + LAG):
         if k < Z:
@@ -404,8 +421,8 @@
     own = None
     for i in zorder:
         zz = zp(i)
-        wait_bytes(rt.at[:, half(zz)], r11.at[i])
-        two = jnp.dot(w_both, rt[:, half(zz)], preferred_element_type=f32)
+        wait_bytes(rt.at[i], r11.at[i])
+        two = jnp.dot(w_both, rt[i], preferred_element_type=f32)
         both = two[:S] + two[S:] + sho[zz] + shr[zz].astype(f32)
         if i:
             fin[i] = both.astype(bf16)
@@ -424,11 +441,11 @@
     wait_bytes(mixo.at[pl.ds(1, Z - 1)], s4)
     wait_bytes(mixo.at[pl.ds(1, Z - 1)], s5)
     wait_bytes(mixs, s6)
-    wait_bytes(disp.at[pl.ds(0, NS - L * ROOM)], s7)
+    wait_bytes(disp.at[:, pl.ds(0, NS - L * ROOM)], s7)
     wait_bytes(disp, s8)
     wait_bytes(shs, s9)
     wait_bytes(po, s10)
-    wait_bytes(ret.at[pl.ds(0, NS - L * ROOM)], s11)
+    wait_bytes(ret.at[:, pl.ds(0, NS - L * ROOM)], s11)
     wait_bytes(fin.at[pl.ds(1, Z - 1)], s12)
     out_mat.wait()
     out_norm.wait()
@@ -465,12 +482,12 @@
         V((E, S, KS), bf16), V((E, S, KS), bf16), V((E, S, 512), bf16), V((E, S, 512), bf16),
         V((HN, 4, S, HD), f32), V((HN, S, HD), f32), V((S, HN * HD), bf16),
         V((Z, S, W), bf16), V((Z, S, W), bf16), V((Z, S, W), f32), V((Z, S, W), bf16), V((Z, S, W), bf16),
-        V((S, W), bf16), V((2, Z, S, W), bf16), V((NS, H), bf16), V((2, NS, H), bf16), V((NS, H), bf16), V((S, H), bf16),
-        V((NS, 512), f32), V((Z, NS, W), bf16), V((Z, NS, W), bf16), V((NS, H), bf16), V((NS, H), bf16),
+        V((S, W), bf16), V((2, Z, S, W), bf16), V((Z, NS, W), bf16), V((2, Z, NS, W), bf16), V((S, H), bf16), V((NS, 512), f32), V((NS, 128), f32),
+        V((Z, NS, W), bf16), V((Z, NS, W), bf16), V((Z, NS, W), bf16), V((Z, NS, W), bf16),
         V((Z, S, W), bf16), V((Z, S, W), bf16), V((Z, S, W), f32), V((Z, S, W), bf16), V((Z, S, W), bf16),
         V(snorm.shape, f32), V((HN, S), f32),
         dma((10,)), dma((6,)), dma((12,)),
-        dma((E,)), dma((1,)), dma((Z,)), dma((1,)), dma((Z,)), dma((1,)), dma((E,)), dma((1,)), dma((1,)), dma((Z,)),
+        dma((E,)), dma((1,)), dma((Z,)), dma((1,)), dma((Z,)), dma((1,)), dma((Z,)), dma((Z,)), dma((1,)), dma((Z,)),
         dma((Z,)), dma((1,)), dma((3,)),
     ]
     anywhere = pl.BlockSpec(memory_space=pl.ANY)

time: 62.8 us -> 60.7 us (0.967)
  Pallas kernels: 62.1 us -> 60 us
    pallas_call x1, Pallas kernels: 60.7 us -> 58.6 us  [per_device(): pl.pallas_call(functools.partial(layer_kernel, (EY, EX, Z, S, D, HD, L)),...]
where the time goes in v4:
time: 60.7 us; the launch traced here: 60.6 us
  Pallas kernels  60 us (99%)
  between operations  0.65 us (1%)
    pallas_call x1, Pallas kernels, per_device(): pl.pallas_call(functools.partial(layer_kernel, (EY, EX, Z, S, D, HD, L)),...  58.6 us
    pallas_call x1, Pallas kernels, per_device(): pl.pallas_call(store_kernel, out_shape=tuple((jax.ShapeDtypeStruct(*r) fo...  1.37 us

profile of v4, /device:TPU:1, one launch (start us, length us, event | category | flops | bytes accessed | tf_op | source)
XLA Modules:
  0.0 60.6 jit_solution(6189025619457569762)
XLA Ops:
  0.6 58.6 %layer.1 = (bf16[32,256]{1,0:T(8,128)(2,1)S(1)}, f32[32,2,64,64]{3,2,1,0:T(8,128)S(1)}, f32[32,2,64]{2,1,0:T(2,128)S(1)}, f32[2,32]{1,0:T(2,128)S(1)}) custom-call(bf16[32,4096]{1,0:T(8,128)(2,1)} %hidden_h.1, f32[1,4096]{1,0:T(1,128)} %bitcast.12, bf16[256,128]{1,0:T(8,128)(2,1)} %wq_h.1, bf16[256,128]{1,0:T(8,128)(2,1)} %wk_h.1, bf16[256,128]{1,0:T(8,128)(2,1)} %wv_h.1, ...), custom_call_target="tpu_custom_call" | custom-call | tf_op jit(solution)/shard_map/layer/pallas_call | solution.py:499
  59.3 1.4 %store.1 = (bf16[32,256]{1,0:T(8,128)(2,1)}, f32[32,2,64,64]{3,2,1,0:T(8,128)}, f32[32,2,64]{2,1,0:T(2,128)}, f32[2,32]{1,0:T(2,128)}) custom-call(bf16[32,256]{1,0:T(8,128)(2,1)S(1)} %get-tuple-element.12.refs_0_, f32[32,2,64,64]{3,2,1,0:T(8,128)S(1)} %get-tuple-element.13.refs_1_, f32[32,2,64]{2,1,0:T(2,128)S(1)} %get-tuple-element.14.refs_2_, ...), custom_call_target="tpu_custom_call" | custom-call | tf_op jit(solution)/shard_map/store/pallas_call | solution.py:510

commit v5 on v4

--- a/solution.py
+++ b/solution.py
@@ -9,9 +9,11 @@
 
 MESH = pl.DeviceIdType.MESH
 NORM_EPS = 1e-06
-ORDER_A = (1, 4, 3, 2)
-ORDER_B = (1, 2, 4, 3)
-ROOM = 4
+CLASSES = (1,), (2,), (4, 3)
+PARTS = 4
+CAP = 3
+PAIRS = 4
+SENT = 3
 
 
 def remote(src, dst, send_sem, recv_sem, dev):
@@ -71,8 +73,8 @@
     xpart = [lax.rem(x + k, EX) for k in range(EX)]
     peers = [None] + [ypart[i // EX] + xpart[i % EX] for i in range(1, E)]
     ep_far = by_hops(EY, EX, (4, 3, 2, 1))
-    ep_sent = by_hops(EY, EX, ORDER_A)
-    ep_done = by_hops(EY, EX, ORDER_B)
+    classes = [k for k in (by_hops(EY, EX, hops) for hops in CLASSES) if k]
+    starts = [1 + sum(len(k) for k in classes[:n]) for n in range(len(classes))]
 
     def z_dev(zz):
         return (e, zz * 2 + c)
@@ -89,8 +91,8 @@
     def half(zz):
         return pl.ds(pl.multiple_of(zz * W, W), W)
 
-    def rows(g):
-        return pl.ds(pl.multiple_of(g * L * ROOM, L * ROOM), L * ROOM)
+    used = pl.ds(0, SENT)
+    GROUP = 2 * PAIRS
 
     def each(first, n, step):
         def one(i, _):
@@ -134,12 +136,9 @@
         xn[k] = (v * scale * mgain[:, k * KS : (k + 1) * KS]).astype(bf16)
     pl.semaphore_wait(barrier, E - 1 + Z - 1 + 1)
 
-    def send_x(i):
-        p = peers[i]
-        remote(xn.at[p], ga.at[e], s1, r1.at[i], (p, t)).start()
-
-    for i in ep_sent:
-        send_x(i)
+    for n, (first, members) in enumerate(zip(starts, classes)):
+        for k, i in enumerate(members):
+            remote(xn.at[peers[i]], ga.at[first + k], s1, r1.at[n], (peers[i], t)).start()
 
     ld_wg = load(wg_h, wg)
     ld_bi = load(bias_h, bias)
@@ -173,17 +172,20 @@
     each(0, T, start_narrow)
     each(0, T, start_wide)
 
+    dx[...] = jnp.zeros_like(dx)
+    rt[...] = jnp.zeros_like(rt)
+
     wait_bytes(wqkvo, bulk.at[0])
     qa[0] = jnp.dot(xn[e], wqkvo[...], preferred_element_type=f32).astype(bf16)
 
-    def project(i):
-        g = ep_src(i)
-        remote(xn.at[g], ga.at[g], s1, r1.at[i], (g, t)).wait_recv()
-        pt[g] = jnp.dot(ga[g], wqkvo[...], preferred_element_type=f32).astype(bf16)
-        remote(pt.at[g], qa.at[i], s2, r2.at[0], (g, t)).start()
-
-    for i in ep_done:
-        project(i)
+    for n, (first, members) in enumerate(zip(starts, classes)):
+        many = len(members)
+        wait_bytes(ga.at[pl.ds(first, many)], r1.at[n])
+        parts = jnp.dot(ga[first : first + many].reshape(many * S, KS), wqkvo[...], preferred_element_type=f32)
+        pt[first : first + many] = parts.astype(bf16).reshape(many, S, 4 * 128)
+        for k, i in enumerate(members):
+            g = ep_src(i)
+            remote(pt.at[first + k], qa.at[first + k], s2, r2.at[n], (g, t)).start()
 
     ld_wg.wait()
     ld_bi.wait()
@@ -223,15 +225,21 @@
     r_row = [jnp.sum(jnp.where(eye, r_col[j], 0.0), 0, keepdims=True) for j in range(2)]
     i0 = lax.broadcasted_iota(jnp.int32, (S, S), 0)
     i1 = lax.broadcasted_iota(jnp.int32, (S, S), 1)
-    NS = E * L * ROOM
+    NS = E * GROUP
+
+    def first_slot(expert):
+        ids = expert.astype(jnp.int32)
+        dev = lax.div(ids, L)
+        return (dev * GROUP + (ids - dev * L) * CAP).astype(f32)
+
     slot_row, slot_col = [], []
     for j in range(2):
         same = jnp.where(r_col[0] == r_row[j], 1.0, 0.0) + jnp.where(r_col[1] == r_row[j], 1.0, 0.0)
         rank_row = jnp.sum(jnp.where(i0 < i1, same, 0.0), 0, keepdims=True)
-        slot_row.append(r_row[j] * ROOM + rank_row)
+        slot_row.append(first_slot(r_row[j]) + rank_row)
         same = jnp.where(r_row[0] == r_col[j], 1.0, 0.0) + jnp.where(r_row[1] == r_col[j], 1.0, 0.0)
         rank_col = jnp.sum(jnp.where(i1 < i0, same, 0.0), -1, keepdims=True)
-        slot_col.append(r_col[j] * ROOM + rank_col)
+        slot_col.append(first_slot(r_col[j]) + rank_col)
     slot_ids = lax.broadcasted_iota(jnp.int32, (NS, S), 0).astype(f32)
     chooser = jnp.where((slot_ids == slot_row[0]) | (slot_ids == slot_row[1]), 1.0, 0.0).astype(bf16)
     rw_v = rw[...]
@@ -244,13 +252,13 @@
 
     ld_sn.wait()
     ld_st.wait()
-    wait_bytes(qa.at[pl.ds(1, E - 1)], r2.at[0])
-    roles = []
-    for k in range(4):
-        total = qa[0, :, k * 128 : (k + 1) * 128].astype(f32)
-        for i in range(1, E):
-            total = total + qa[i, :, k * 128 : (k + 1) * 128].astype(f32)
-        roles.append(total.astype(bf16).astype(f32))
+    roles = [qa[0, :, k * 128 : (k + 1) * 128].astype(f32) for k in range(4)]
+    for n, (first, members) in enumerate(zip(starts, classes)):
+        wait_bytes(qa.at[pl.ds(first, len(members))], r2.at[n])
+        for k in range(4):
+            for i in range(first, first + len(members)):
+                roles[k] = roles[k] + qa[i, :, k * 128 : (k + 1) * 128].astype(f32)
+    roles = [r.astype(bf16).astype(f32) for r in roles]
 
     for h in range(HN):
         hs = slice(h * HD, (h + 1) * HD)
@@ -261,24 +269,22 @@
         kvq[h, 3] = jnp.broadcast_to(fws[h], (S, HD))
     SB = 8
 
-    def cell(b):
-        at = pl.ds(pl.multiple_of(b * SB, SB), SB)
+    def seqs(b):
+        return pl.ds(pl.multiple_of(b * SB, SB), SB)
+
+    def read(b):
         for h in range(HN):
-            new = (
-                kvq[h, 3, at, :][:, None, :] * state[at, h]
-                + kvq[h, 2, at, :][:, :, None] * kvq[h, 1, at, :][:, None, :]
-            )
-            state[at, h] = new
-            nums[h, at, :] = jnp.sum(new * kvq[h, 0, at, :][:, None, :], -1)
-
-    each(0, S // SB, cell)
+            nums[h, seqs(b), :] = jnp.sum(state[seqs(b), h] * kvq[h, 0, seqs(b), :][:, None, :], -1)
+
+    each(0, S // SB, read)
     for h in range(HN):
         hs = slice(h * HD, (h + 1) * HD)
         nn = fws[h] * snorm[:, h, :] + iws[h] * kvq[h, 1]
         nnew[:, h, :] = nn
         den = jnp.maximum(jnp.abs(jnp.sum(nn * kvq[h, 0], -1, keepdims=True)), 1.0)
         gate = 1.0 / (1.0 + jnp.exp(-roles[3][:, hs]))
-        gated[:, hs] = (gate * nums[h] / den).astype(bf16)
+        num = fws[h] * nums[h] + kvq[h, 2] * jnp.sum(kvq[h, 1] * kvq[h, 0], -1, keepdims=True)
+        gated[:, hs] = (gate * num / den).astype(bf16)
 
     wait_bytes(wmix, bulk.at[1])
     gv = gated[...]
@@ -286,21 +292,29 @@
     theirs = jnp.dot(gv, wmix[o], preferred_element_type=f32)
     for zz in range(Z):
         mixs[zz] = theirs[:, zz * W : (zz + 1) * W].astype(bf16)
-    for i in zorder:
-        remote(mixs.at[zp(i)], mixr.at[zp(i)], s3, r3.at[i], sib).start()
+    remote(mixs, mixr, s3, r3.at[0], sib).start()
     mine = jnp.dot(gv, wmix[c], preferred_element_type=f32)
     for zz in range(Z):
         mixm[zz] = mine[:, zz * W : (zz + 1) * W]
     own = None
+    remote(mixs, mixr, s3, r3.at[0], sib).wait_recv()
     for i in zorder:
         zz = zp(i)
-        remote(mixs.at[zz], mixr.at[zz], s3, r3.at[i], sib).wait_recv()
         both = mixm[zz] + mixr[zz].astype(f32)
         if i:
             mixo[i] = both.astype(bf16)
             remote(mixo.at[i], rz.at[i], s4, r4.at[0], z_dev(zz)).start()
         else:
             own = both
+
+    def update(b):
+        for h in range(HN):
+            state[seqs(b), h] = (
+                kvq[h, 3, seqs(b), :][:, None, :] * state[seqs(b), h]
+                + kvq[h, 2, seqs(b), :][:, :, None] * kvq[h, 1, seqs(b), :][:, None, :]
+            )
+
+    each(0, S // SB, update)
     out_mat = pltpu.make_async_copy(state, newmat_o, osem.at[0])
     out_mat.start()
     out_norm = pltpu.make_async_copy(nnew, newnorm_o, osem.at[1])
@@ -316,10 +330,10 @@
 
     def dispatch(block, i):
         g = zs(i)
-        disp[g] = jnp.dot(chooser, block, preferred_element_type=f32).astype(bf16)
+        disp[g] = jnp.dot(chooser, block, preferred_element_type=f32).astype(bf16).reshape(E, PAIRS, 2, W)
         for k in ep_far:
-            remote(disp.at[g, rows(peers[k])], dx.at[c, g, rows(e)], s7, r7.at[i], (peers[k], t)).start()
-        pltpu.make_async_copy(disp.at[g, rows(e)], dx.at[c, g, rows(e)], r7.at[i]).start()
+            remote(disp.at[g, peers[k], used], dx.at[c, g, e, used], s7, r7.at[i], (peers[k], t)).start()
+        pltpu.make_async_copy(disp.at[g, e, used], dx.at[c, g, e, used], r7.at[i]).start()
 
     dispatch(so[...], 0)
     remote(so, st.at[c, z], s6, r6.at[0], sib).start()
@@ -361,7 +375,7 @@
     sqs[...] = jnp.zeros_like(sqs)
 
     def block_of(cc, g):
-        v = dx[cc, g].astype(f32)
+        v = dx[cc, g].reshape(NS, W).astype(f32)
         scaled = (v * fgain[:, col(g, cc)]).astype(bf16)
         acc[...] += jnp.dot(scaled, wcat[cc, half(g), :], preferred_element_type=f32)
         v = v * v
@@ -373,7 +387,7 @@
         if k < Z:
             i = arrivals[k]
             g = zs(i)
-            wait_bytes(dx.at[c, g], r7.at[i])
+            wait_bytes(dx.at[c, g, :, used], r7.at[i])
             remote(dx.at[c, g], dx.at[c, g], s8, r8.at[i], sib).start()
             block_of(c, g)
         if k >= BEHIND:
@@ -383,7 +397,7 @@
             block_of(o, g)
     sq = sqs[...]
     escale = lax.rsqrt(jnp.sum(sq, -1, keepdims=True) * (1.0 / D) + NORM_EPS)
-    expert_of = lax.rem(lax.div(lax.broadcasted_iota(jnp.int32, (NS, 128), 0), ROOM), L)
+    expert_of = lax.div(lax.rem(lax.broadcasted_iota(jnp.int32, (NS, 128), 0), GROUP), CAP)
     hids = []
     for j in range(L):
         gv = acc[:, 2 * j * 128 : (2 * j + 1) * 128] * escale
@@ -403,13 +417,13 @@
         zz = zp(i)
         part = jnp.dot(hcat, down[c, :, half(zz)], preferred_element_type=f32)
         remote(po.at[i], pi.at[i], s10, r10.at[i], sib).wait_recv()
-        ret[i] = (part + pi[i].astype(f32)).astype(bf16)
+        ret[i] = (part + pi[i].astype(f32)).astype(bf16).reshape(E, PAIRS, 2, W)
 
         for k in ep_far:
             p = peers[k]
-            remote(ret.at[i, rows(p)], rt.at[i, rows(e)], s11, r11.at[i], (p, t)).start()
-
-        pltpu.make_async_copy(ret.at[i, rows(e)], rt.at[i, rows(e)], r11.at[i]).start()
+            remote(ret.at[i, p, used], rt.at[i, e, used], s11, r11.at[i], (p, t)).start()
+
+        pltpu.make_async_copy(ret.at[i, e, used], rt.at[i, e, used], r11.at[i]).start()
 
     for k in range(Z + LAG):
         if k < Z:
@@ -421,8 +435,8 @@
     own = None
     for i in zorder:
         zz = zp(i)
-        wait_bytes(rt.at[i], r11.at[i])
-        two = jnp.dot(w_both, rt[i], preferred_element_type=f32)
+        wait_bytes(rt.at[i, :, used], r11.at[i])
+        two = jnp.dot(w_both, rt[i].reshape(NS, W), preferred_element_type=f32)
         both = two[:S] + two[S:] + sho[zz] + shr[zz].astype(f32)
         if i:
             fin[i] = both.astype(bf16)
@@ -441,11 +455,11 @@
     wait_bytes(mixo.at[pl.ds(1, Z - 1)], s4)
     wait_bytes(mixo.at[pl.ds(1, Z - 1)], s5)
     wait_bytes(mixs, s6)
-    wait_bytes(disp.at[:, pl.ds(0, NS - L * ROOM)], s7)
+    wait_bytes(disp.at[:, pl.ds(0, E - 1), used], s7)
     wait_bytes(disp, s8)
     wait_bytes(shs, s9)
     wait_bytes(po, s10)
-    wait_bytes(ret.at[:, pl.ds(0, NS - L * ROOM)], s11)
+    wait_bytes(ret.at[:, pl.ds(0, E - 1), used], s11)
     wait_bytes(fin.at[pl.ds(1, Z - 1)], s12)
     out_mat.wait()
     out_norm.wait()
@@ -455,7 +469,11 @@
 def store_kernel(*refs):
     n = len(refs) // 2
     sem = refs[-1]
-    copies = [pltpu.make_async_copy(refs[i], refs[n + i], sem.at[i]) for i in range(n)]
+    copies = [pltpu.make_async_copy(refs[i], refs[n + i], sem.at[i]) for i in range(n) if i != 1]
+    part = refs[1].shape[0] // PARTS
+    for k in range(PARTS):
+        some = pl.ds(k * part, part)
+        copies.append(pltpu.make_async_copy(refs[1].at[some], refs[n + 1].at[some], sem.at[n + k]))
     for cp in copies:
         cp.start()
     for cp in copies:
@@ -470,7 +488,7 @@
     S, D = hidden.shape
     HN, HD = state.shape[1], state.shape[2]
     L, SW = eg.shape[0], sg.shape[1]
-    W, KS, NS = D // T, D // E, E * L * ROOM
+    W, KS, NS = D // T, D // E, E * 2 * PAIRS
     f32, bf16 = jnp.float32, jnp.bfloat16
     V, dma = pltpu.VMEM, pltpu.SemaphoreType.DMA
     H = D // 2
@@ -482,12 +500,12 @@
         V((E, S, KS), bf16), V((E, S, KS), bf16), V((E, S, 512), bf16), V((E, S, 512), bf16),
         V((HN, 4, S, HD), f32), V((HN, S, HD), f32), V((S, HN * HD), bf16),
         V((Z, S, W), bf16), V((Z, S, W), bf16), V((Z, S, W), f32), V((Z, S, W), bf16), V((Z, S, W), bf16),
-        V((S, W), bf16), V((2, Z, S, W), bf16), V((Z, NS, W), bf16), V((2, Z, NS, W), bf16), V((S, H), bf16), V((NS, 512), f32), V((NS, 128), f32),
-        V((Z, NS, W), bf16), V((Z, NS, W), bf16), V((Z, NS, W), bf16), V((Z, NS, W), bf16),
+        V((S, W), bf16), V((2, Z, S, W), bf16), V((Z, E, PAIRS, 2, W), bf16), V((2, Z, E, PAIRS, 2, W), bf16), V((S, H), bf16), V((NS, 512), f32), V((NS, 128), f32),
+        V((Z, NS, W), bf16), V((Z, NS, W), bf16), V((Z, E, PAIRS, 2, W), bf16), V((Z, E, PAIRS, 2, W), bf16),
         V((Z, S, W), bf16), V((Z, S, W), bf16), V((Z, S, W), f32), V((Z, S, W), bf16), V((Z, S, W), bf16),
         V(snorm.shape, f32), V((HN, S), f32),
         dma((10,)), dma((6,)), dma((12,)),
-        dma((E,)), dma((1,)), dma((Z,)), dma((1,)), dma((Z,)), dma((1,)), dma((Z,)), dma((Z,)), dma((1,)), dma((Z,)),
+        dma((3,)), dma((3,)), dma((1,)), dma((1,)), dma((Z,)), dma((1,)), dma((Z,)), dma((Z,)), dma((1,)), dma((Z,)),
         dma((Z,)), dma((1,)), dma((3,)),
     ]
     anywhere = pl.BlockSpec(memory_space=pl.ANY)
@@ -512,7 +530,7 @@
         out_shape=tuple(jax.ShapeDtypeStruct(*r) for r in results),
         in_specs=[anywhere] * len(results),
         out_specs=(anywhere,) * len(results),
-        scratch_shapes=[dma((len(results),))],
+        scratch_shapes=[dma((len(results) + PARTS,))],
         compiler_params=pltpu.CompilerParams(vmem_limit_bytes=1024 * 1024),
         name="store",
     )(*(pltpu.with_memory_space_constraint(a, V) for a in inner))

time: 60.7 us -> 58.3 us (0.960)
  Pallas kernels: 60 us -> 57.6 us
    pallas_call x1, Pallas kernels: 58.6 us -> 56.2 us  [per_device(): pl.pallas_call(functools.partial(layer_kernel, (EY, EX, Z, S, D, HD, L)),...]
where the time goes in v5:
time: 58.3 us; the launch traced here: 58.2 us
  Pallas kernels  57.6 us (99%)
  between operations  0.65 us (1%)
    pallas_call x1, Pallas kernels, per_device(): pl.pallas_call(functools.partial(layer_kernel, (EY, EX, Z, S, D, HD, L)),...  56.2 us
    pallas_call x1, Pallas kernels, per_device(): pl.pallas_call(store_kernel, out_shape=tuple((jax.ShapeDtypeStruct(*r) fo...  1.4 us

profile of v5, /device:TPU:1, one launch (start us, length us, event | category | flops | bytes accessed | tf_op | source)
XLA Modules:
  0.0 58.2 jit_solution(3461462894520591972)
XLA Ops:
  0.6 56.2 %layer.1 = (bf16[32,256]{1,0:T(8,128)(2,1)S(1)}, f32[32,2,64,64]{3,2,1,0:T(8,128)S(1)}, f32[32,2,64]{2,1,0:T(2,128)S(1)}, f32[2,32]{1,0:T(2,128)S(1)}) custom-call(bf16[32,4096]{1,0:T(8,128)(2,1)} %hidden_h.1, f32[1,4096]{1,0:T(1,128)} %bitcast.12, bf16[256,128]{1,0:T(8,128)(2,1)} %wq_h.1, bf16[256,128]{1,0:T(8,128)(2,1)} %wk_h.1, bf16[256,128]{1,0:T(8,128)(2,1)} %wv_h.1, ...), custom_call_target="tpu_custom_call" | custom-call | tf_op jit(solution)/shard_map/layer/pallas_call | solution.py:517
  56.8 1.4 %store.1 = (bf16[32,256]{1,0:T(8,128)(2,1)}, f32[32,2,64,64]{3,2,1,0:T(8,128)}, f32[32,2,64]{2,1,0:T(2,128)}, f32[2,32]{1,0:T(2,128)}) custom-call(bf16[32,256]{1,0:T(8,128)(2,1)S(1)} %get-tuple-element.12.refs_0_, f32[32,2,64,64]{3,2,1,0:T(8,128)S(1)} %get-tuple-element.13.refs_1_, f32[32,2,64]{2,1,0:T(2,128)S(1)} %get-tuple-element.14.refs_2_, ...), custom_call_target="tpu_custom_call" | custom-call | tf_op jit(solution)/shard_map/store/pallas_call | solution.py:528

commit v6 on v5

--- a/solution.py
+++ b/solution.py
@@ -388,12 +388,12 @@
             i = arrivals[k]
             g = zs(i)
             wait_bytes(dx.at[c, g, :, used], r7.at[i])
-            remote(dx.at[c, g], dx.at[c, g], s8, r8.at[i], sib).start()
+            remote(dx.at[c, g, :, used], dx.at[c, g, :, used], s8, r8.at[i], sib).start()
             block_of(c, g)
         if k >= BEHIND:
             i = arrivals[k - BEHIND]
             g = zs(i)
-            remote(dx.at[c, g], dx.at[o, g], s8, r8.at[i], sib).wait_recv()
+            wait_bytes(dx.at[o, g, :, used], r8.at[i])
             block_of(o, g)
     sq = sqs[...]
     escale = lax.rsqrt(jnp.sum(sq, -1, keepdims=True) * (1.0 / D) + NORM_EPS)
@@ -456,7 +456,7 @@
     wait_bytes(mixo.at[pl.ds(1, Z - 1)], s5)
     wait_bytes(mixs, s6)
     wait_bytes(disp.at[:, pl.ds(0, E - 1), used], s7)
-    wait_bytes(disp, s8)
+    wait_bytes(disp.at[:, :, used], s8)
     wait_bytes(shs, s9)
     wait_bytes(po, s10)
     wait_bytes(ret.at[:, pl.ds(0, E - 1), used], s11)

time: 58.3 us -> 58 us (level)
  no operation moved by 1% of the time
where the time goes in v6:
time: 58 us; the launch traced here: 57.9 us
  Pallas kernels  57.3 us (99%)
  between operations  0.65 us (1%)
    pallas_call x1, Pallas kernels, per_device(): pl.pallas_call(functools.partial(layer_kernel, (EY, EX, Z, S, D, HD, L)),...  55.9 us
    pallas_call x1, Pallas kernels, per_device(): pl.pallas_call(store_kernel, out_shape=tuple((jax.ShapeDtypeStruct(*r) fo...  1.4 us

profile of v6, /device:TPU:1, one launch (start us, length us, event | category | flops | bytes accessed | tf_op | source)
XLA Modules:
  0.0 57.9 jit_solution(11349030858250692448)
XLA Ops:
  0.6 55.9 %layer.1 = (bf16[32,256]{1,0:T(8,128)(2,1)S(1)}, f32[32,2,64,64]{3,2,1,0:T(8,128)S(1)}, f32[32,2,64]{2,1,0:T(2,128)S(1)}, f32[2,32]{1,0:T(2,128)S(1)}) custom-call(bf16[32,4096]{1,0:T(8,128)(2,1)} %hidden_h.1, f32[1,4096]{1,0:T(1,128)} %bitcast.12, bf16[256,128]{1,0:T(8,128)(2,1)} %wq_h.1, bf16[256,128]{1,0:T(8,128)(2,1)} %wk_h.1, bf16[256,128]{1,0:T(8,128)(2,1)} %wv_h.1, ...), custom_call_target="tpu_custom_call" | custom-call | tf_op jit(solution)/shard_map/layer/pallas_call | solution.py:517
  56.5 1.4 %store.1 = (bf16[32,256]{1,0:T(8,128)(2,1)}, f32[32,2,64,64]{3,2,1,0:T(8,128)}, f32[32,2,64]{2,1,0:T(2,128)}, f32[2,32]{1,0:T(2,128)}) custom-call(bf16[32,256]{1,0:T(8,128)(2,1)S(1)} %get-tuple-element.12.refs_0_, f32[32,2,64,64]{3,2,1,0:T(8,128)S(1)} %get-tuple-element.13.refs_1_, f32[32,2,64]{2,1,0:T(2,128)S(1)} %get-tuple-element.14.refs_2_, ...), custom_call_target="tpu_custom_call" | custom-call | tf_op jit(solution)/shard_map/store/pallas_call | solution.py:528
